TPU v7x, 512 devices: a whole 4x8x8 slice. The times are simulated.
512 devices in a mesh: rep: 64 (over z, y), fs: 4 (over x), tp: 2 (over core).
Axes of the slice: x: 4, y: 8, z: 8, core: 2. Of those that a mesh axis runs over, the one named last changes fastest.
Arguments:
- inputs: bfloat16 [8192, 2048], P(('rep', 'fs', 'tp')), may hold values from -6 to 6
- cotangent: bfloat16 [8192, 2048], P(('rep', 'fs', 'tp')), may hold values from -24 to 24
- norm_gain: float32 [2048], replicated, may hold values from 0.1 to 1.9
- gate_weight: bfloat16 [2048, 2816], P(None, ('fs', 'tp')), may hold values from -0.125 to 0.125
- up_weight: bfloat16 [2048, 2816], P(None, ('fs', 'tp')), may hold values from -0.125 to 0.125
- down_weight: bfloat16 [2816, 2048], P(('fs', 'tp')), may hold values from -0.109375 to 0.109375
Outputs:
- input_grad: bfloat16 [8192, 2048], P(('rep', 'fs', 'tp'))
- gain_grad: float32 [2048], replicated
- down_grad: float32 [2816, 2048], P(('fs', 'tp'), 'rep')
All inputs are finite; a program needn't handle non-finite values.
Results may differ from a plain program's by a relative error of at most 0.0066.
Values may be sent and summed in bfloat16 or wider, within the bound.
No kernel may reach another device: no remote copies, remote signals or barrier semaphores. Data moves between devices by JAX's collectives and lax.ppermute only.
A program may use at most 64 MiB of HBM per device.

v0:
```python
import functools

import jax
import jax.numpy as jnp
from jax import lax
from jax.sharding import Mesh
from jax.sharding import PartitionSpec as P

REP_FS_TP = ("rep_0", "rep_1", "fs", "tp")
REP = ("rep_0", "rep_1")


EPS = 1e-06


def from_everyone(array, axis):
    count = lax.axis_size(axis)
    return lax.all_to_all(
        jnp.broadcast_to(array[None], (count, *array.shape)), axis, 0, 0, tiled=True
    )


def laid_out(parts, dim):
    dims = list(parts.shape[1:])
    dims[dim] *= parts.shape[0]
    return jnp.moveaxis(parts, 0, dim).reshape(dims)


def gathered_copies(array, axis, dim):
    parts = from_everyone(array, axis)
    return laid_out(parts, dim)


def sent_together(arrays, axis, dim, along):
    widths = [a.shape[along] for a in arrays]
    both = jnp.concatenate(arrays, axis=along)
    result = gathered_copies(both, axis, dim)
    return tuple(jnp.split(result, [sum(widths[:k]) for k in range(1, len(widths))], axis=along))


def in_blocks(array, dim, count):
    dims = array.shape
    parts = array.reshape(*dims[:dim], count, dims[dim] // count, *dims[dim + 1 :])
    return jnp.moveaxis(parts, dim, 0)


def sent_and_summed(array, axis, dim):
    count = lax.axis_size(axis)
    parts = lax.all_to_all(in_blocks(array, dim, count), axis, 0, 0, tiled=True)
    return jnp.sum(parts.astype(jnp.float32), axis=0)


def one_axis_at_a_time(array, axes):
    return functools.reduce(lax.psum, axes, array)


def cut_rows(length, count):
    step = length // count
    if step >= 8:
        step -= step % 8
    return [step * k for k in range(1, count)]


def exchange_in_pieces(array, axis, pieces, split_dim, concat_dim):
    parts = in_blocks(array, split_dim, lax.axis_size(axis))
    cut = max(range(1, max(2, parts.ndim - 1)), key=lambda d: parts.shape[d])
    outs = []
    for slab in jnp.split(parts, cut_rows(parts.shape[cut], pieces), axis=cut):
        if slab.size:
            outs.append(lax.all_to_all(slab, axis, split_axis=0, concat_axis=0, tiled=True))
    return laid_out(jnp.concatenate(outs, axis=cut), concat_dim)


def across_tokens(left, right):
    return lax.dot_general(
        left, right, (((0,), (0,)), ((), ())), preferred_element_type=jnp.float32
    )


def across_columns(left, right):
    return lax.dot_general(
        left, right, (((1,), (1,)), ((), ())), preferred_element_type=jnp.float32
    )


def per_device(inputs, cotangent, norm_gain, gate_weight, up_weight, down_weight):
    whole_x, whole_dy = sent_together((inputs, cotangent), ("fs", "tp"), 0, 1)
    xf = whole_x.astype(jnp.float32)
    inv = lax.rsqrt(jnp.mean(xf * xf, axis=-1, keepdims=True) + EPS)
    normed = xf * inv
    hidden_in = (normed * norm_gain).astype(jnp.bfloat16)
    gate = jnp.dot(hidden_in, gate_weight, preferred_element_type=jnp.float32)
    up = jnp.dot(hidden_in, up_weight, preferred_element_type=jnp.float32)
    sig = jax.nn.sigmoid(gate)
    act = gate * sig
    hidden = (act * up).astype(jnp.bfloat16)
    d_hidden = 0.5 * across_columns(whole_dy, down_weight)
    d_gate = (d_hidden * up * sig * (1.0 + gate * (1.0 - sig))).astype(jnp.bfloat16)
    d_up = (d_hidden * act).astype(jnp.bfloat16)
    own_rows = inputs.shape[0]
    d_in = sent_and_summed(
        (across_columns(d_gate, gate_weight) + across_columns(d_up, up_weight)).astype(
            jnp.bfloat16
        ),
        ("fs", "tp"),
        0,
    )
    offset = lax.axis_index(("fs", "tp")) * own_rows
    own_normed = lax.dynamic_slice_in_dim(normed, offset, own_rows, 0)
    own_inv = lax.dynamic_slice_in_dim(inv, offset, own_rows, 0)
    gain_grad = one_axis_at_a_time(jnp.sum(d_in * own_normed, axis=0), REP_FS_TP)
    scaled = d_in * norm_gain
    input_grad = (
        own_inv * (scaled - own_normed * jnp.mean(scaled * own_normed, axis=-1, keepdims=True))
    ).astype(jnp.bfloat16)
    input_grad, gain_grad = (input_grad, gain_grad)
    part_down = 0.5 * across_tokens(whole_dy, hidden)
    got_down = exchange_in_pieces(part_down[None].astype(jnp.bfloat16), REP, 2, 1, 0).astype(
        jnp.float32
    )
    down_grad = jnp.sum(got_down, axis=0).T
    return (input_grad, gain_grad, down_grad)


def solution(mesh):
    finer = Mesh(
        mesh.devices.reshape(8, 8, mesh.shape["fs"], mesh.shape["tp"]),
        ("rep_0", "rep_1", "fs", "tp"),
    )
    placed = (
        P(REP_FS_TP, None),
        P(REP_FS_TP, None),
        P(),
        P(None, ("fs", "tp")),
        P(None, ("fs", "tp")),
        P(("fs", "tp"), None),
    )
    return jax.shard_map(
        per_device,
        mesh=finer,
        in_specs=placed,
        out_specs=(P(REP_FS_TP, None), P(), P(("fs", "tp"), REP)),
        check_vma=False,
    )
```

profile of v0, /device:TPU:1, one launch (start us, length us, event | category | flops | bytes accessed | tf_op | source)
XLA Modules:
  0.0 148.0 jit_solution(1955970298010030403)
XLA Ops:
  0.6 1.0 pad_maximum_fusion
  1.8 24.3 %all_to_all.20 = bf16[8,16,4096]{2,1,0:T(8,128)(2,1)S(1)} all-to-all(bf16[8,16,4096]{2,1,0:T(8,128)(2,1)S(1)} %broadcast_in_dim.2), channel_id=1, replica_groups=mesh['rep_0'=8,'rep_1'=8,'fs'=4,'tp'=2] {'fs','tp'}, dimensions={0} | all-to-all | bytes 2097152 | tf_op jit(solution)/shard_map/all_to_all | solution.py:18
  26.3 0.5 convolution_multiply_fusion.1
  26.9 0.6 fusion.5
  27.5 0.7 copy-done.4
  28.2 0.6 fusion.6
  29.4 1.3 fusion.1
  30.7 4.4 %all-to-all-start.1 = ((bf16[8,16,2048]{2,1,0:T(8,128)(2,1)}), bf16[8,16,2048]{2,1,0:T(8,128)(2,1)S(1)}, u32[]{:S(2)}, u32[]{:S(2)}) async-start(bf16[8,16,2048]{2,1,0:T(8,128)(2,1)} %bitcast.1), calls=%async_computation.1 | async-start | bytes 1048576 | tf_op jit(solution)/shard_map/all_to_all | solution.py:49
  35.1 1.6 %fusion = bf16[2048,352]{0,1:T(8,128)(2,1)} fusion(bf16[128,4096]{1,0:T(8,128)(2,1)S(1)} %bitcast.17, f32[128,352]{0,1:T(8,128)S(1)} %fusion.6, f32[128,352]{0,1:T(8,128)S(1)} %fusion.5), kind=kOutput, calls=%fused_computation.2 | convolution fusion | flops 186261504 | bytes 2326528 | tf_op jit(solution)/shard_map/dot_general | solution.py:75
  36.8 2.6 %copy.10 = bf16[2048,352]{1,0:T(8,128)(2,1)} copy(bf16[2048,352]{0,1:T(8,128)(2,1)} %fusion) | data formatting | bytes 2883584 | tf_op jit(solution)/shard_map/convert_element_type | solution.py:118
  39.3 2.7 %slice_bitcast_fusion.1 = (bf16[64,1,16,352]{3,2,1,0:T(8,128)(2,1)}, bf16[64,1,16,352]{3,2,1,0:T(8,128)(2,1)}) fusion(bf16[64,1,32,352]{3,2,0,1:T(8,128)(2,1)} %bitcast.19), kind=kLoop, calls=%fused_computation.12 | loop fusion | bytes 2883584 | tf_op jit(solution)/shard_map/split | solution.py:68
  42.0 2.5 %all-to-all-done.1 = bf16[8,16,2048]{2,1,0:T(8,128)(2,1)S(1)} async-done(((bf16[8,16,2048]{2,1,0:T(8,128)(2,1)}), bf16[8,16,2048]{2,1,0:T(8,128)(2,1)S(1)}, u32[]{:S(2)}, u32[]{:S(2)}) %all-to-all-start.1) | async-done | bytes 524320 | tf_op jit(solution)/shard_map/all_to_all | solution.py:49
  44.5 0.8 copy-done.1
  45.3 12.6 %all-to-all-start.3 = ((bf16[64,1,16,352]{3,2,1,0:T(8,128)(2,1)}), bf16[64,1,16,352]{3,2,1,0:T(8,128)(2,1)S(1)}, u32[]{:S(2)}, u32[]{:S(2)}) async-start(bf16[64,1,16,352]{3,2,1,0:T(8,128)(2,1)} %get-tuple-element.6), calls=%async_computation.3 | async-start | bytes 1572864 | tf_op jit(solution)/shard_map/all_to_all | solution.py:70
  58.0 21.4 %all-to-all-done.3 = bf16[64,1,16,352]{3,2,1,0:T(8,128)(2,1)S(1)} async-done(((bf16[64,1,16,352]{3,2,1,0:T(8,128)(2,1)}), bf16[64,1,16,352]{3,2,1,0:T(8,128)(2,1)S(1)}, u32[]{:S(2)}, u32[]{:S(2)}) %all-to-all-start.3) | async-done | bytes 720928 | tf_op jit(solution)/shard_map/all_to_all | solution.py:70
  79.4 8.2 %all-to-all-start.2 = ((bf16[64,1,16,352]{3,2,1,0:T(8,128)(2,1)}), bf16[64,1,16,352]{3,2,1,0:T(8,128)(2,1)}, u32[]{:S(2)}, u32[]{:S(2)}) async-start(bf16[64,1,16,352]{3,2,1,0:T(8,128)(2,1)} %get-tuple-element.5), calls=%async_computation.2 | async-start | bytes 1572864 | tf_op jit(solution)/shard_map/all_to_all | solution.py:70
  87.8 0.9 copy-done.2
  88.7 0.9 copy-done.3
  89.8 22.1 %psum.28 = f32[2048]{0:T(1024)S(1)} all-reduce(f32[2048]{0:T(1024)S(1)} %get-tuple-element.3), channel_id=1, replica_groups=mesh['rep_0'=8,'rep_1'=8,'fs'=4,'tp'=2] {'rep_0'}, use_global_device_ids=true, to_apply=%region_4.0 | all-reduce | flops 2048 | bytes 16384 | tf_op jit(solution)/shard_map/psum | solution.py:54
  111.9 13.8 %psum.29 = f32[2048]{0:T(1024)S(1)} all-reduce(f32[2048]{0:T(1024)S(1)} %psum.28), channel_id=1, replica_groups=mesh['rep_0'=8,'rep_1'=8,'fs'=4,'tp'=2] {'rep_1'}, use_global_device_ids=true, to_apply=%region_5.0 | all-reduce | flops 2048 | bytes 16384 | tf_op jit(solution)/shard_map/psum | solution.py:54
  125.7 7.0 %psum.30 = f32[2048]{0:T(1024)S(1)} all-reduce(f32[2048]{0:T(1024)S(1)} %psum.29), channel_id=1, replica_groups=mesh['rep_0'=8,'rep_1'=8,'fs'=4,'tp'=2] {'fs'}, use_global_device_ids=true, to_apply=%region_6.0 | all-reduce | flops 2048 | bytes 16384 | tf_op jit(solution)/shard_map/psum | solution.py:54
  132.7 11.6 %psum.31 = f32[2048]{0:T(1024)} all-reduce(f32[2048]{0:T(1024)S(1)} %psum.30), channel_id=1, replica_groups=mesh['rep_0'=8,'rep_1'=8,'fs'=4,'tp'=2] {'tp'}, use_global_device_ids=true, to_apply=%region_7.0 | all-reduce | flops 2048 | bytes 16384 | tf_op jit(solution)/shard_map/psum | solution.py:54
  144.3 1.6 %multiply_convert_fusion.6 = bf16[16,2048]{1,0:T(8,128)(2,1)} fusion(f32[16,2048]{1,0:T(8,128)S(1)} %convert_reduce_fusion.1, f32[128,2048]{1,0:T(8,128)} %copy-done.3, s32[]{:T(128)S(6)} %select_n.4, f32[16]{0:T(128)S(1)} %broadcast_multiply_fusion, f32[2048]{0:T(1024)S(1)} %copy-done.6, f32[16]{0:T(128)S(1)} %dynamic-slice.3), kind=kLoop, calls=%fused_computation.24 | loop fusion | flops 163840 | bytes 336004 | tf_op jit(solution)/shard_map/convert_element_type | solution.py:115
  146.0 2.1 %convert_reduce_fusion = f32[32,352]{1,0:T(8,128)} fusion(bf16[64,1,16,352]{3,2,1,0:T(8,128)(2,1)S(1)} %all-to-all-done.3, bf16[64,1,16,352]{3,2,1,0:T(8,128)(2,1)} %all-to-all-done.2), kind=kLoop, calls=%fused_computation | loop fusion | flops 3593216 | bytes 1486848 | tf_op jit(solution)/shard_map/reduce_sum | solution.py:121
  (20 shorter events, 1.3 us)
Async XLA Ops:
  0.6 26.2 %copy-start = (bf16[2048,352]{0,1:T(8,128)(2,1)S(1)}, bf16[2048,352]{0,1:T(8,128)(2,1)}, u32[]{:S(2)}) copy-start(bf16[2048,352]{0,1:T(8,128)(2,1)} %param.9) | copy-start | bytes 4325380
  1.7 24.5 %copy-start.5 = (bf16[352,2048]{1,0:T(8,128)(2,1)S(1)}, bf16[352,2048]{1,0:T(8,128)(2,1)}, u32[]{:S(2)}) copy-start(bf16[352,2048]{1,0:T(8,128)(2,1)} %param.11) | copy-start | bytes 4325380
  26.1 0.8 copy-start.6
  26.9 1.4 copy-start.4
  30.7 13.8 %all-to-all-start.1 = ((bf16[8,16,2048]{2,1,0:T(8,128)(2,1)}), bf16[8,16,2048]{2,1,0:T(8,128)(2,1)S(1)}, u32[]{:S(2)}, u32[]{:S(2)}) async-start(bf16[8,16,2048]{2,1,0:T(8,128)(2,1)} %bitcast.1), calls=%async_computation.1 | async-start | bytes 1048576 | tf_op jit(solution)/shard_map/all_to_all | solution.py:49
  44.5 0.8 copy-start.1
  45.3 34.1 %all-to-all-start.3 = ((bf16[64,1,16,352]{3,2,1,0:T(8,128)(2,1)}), bf16[64,1,16,352]{3,2,1,0:T(8,128)(2,1)S(1)}, u32[]{:S(2)}, u32[]{:S(2)}) async-start(bf16[64,1,16,352]{3,2,1,0:T(8,128)(2,1)} %get-tuple-element.6), calls=%async_computation.3 | async-start | bytes 1572864 | tf_op jit(solution)/shard_map/all_to_all | solution.py:70
  79.4 66.6 %all-to-all-start.2 = ((bf16[64,1,16,352]{3,2,1,0:T(8,128)(2,1)}), bf16[64,1,16,352]{3,2,1,0:T(8,128)(2,1)}, u32[]{:S(2)}, u32[]{:S(2)}) async-start(bf16[64,1,16,352]{3,2,1,0:T(8,128)(2,1)} %get-tuple-element.5), calls=%async_computation.2 | async-start | bytes 1572864 | tf_op jit(solution)/shard_map/all_to_all | solution.py:70
  87.6 1.0 copy-start.2
  88.7 1.0 copy-start.3
where the time goes:
time: 149 us; the launch traced here: 148 us
  blocking collectives  78.8 us (53%)
  starting transfers between devices  25.3 us (17%)
  waiting for transfers between devices  23.8 us (16%)
  local copies, waits for them, and re-layouts  8.79 us (6%)
  other arithmetic  5.23 us (4%)
  matrix products  5.23 us (4%)
    psum x4, blocking collectives, one_axis_at_a_time(): return functools.reduce(lax.psum, axes, array)  54.5 us
    all_to_all x1, blocking collectives, from_everyone(): lax.all_to_all(jnp.broadcast_to(array[None], (count, *array.shape)), axis...  24.3 us
    all_to_all x2, waiting for transfers between devices, exchange_in_pieces(): lax.all_to_all(slab, axis, split_axis=0, concat_axis=0, tiled=True)  21.4 us
    all_to_all x2, starting transfers between devices, exchange_in_pieces(): lax.all_to_all(slab, axis, split_axis=0, concat_axis=0, tiled=True)  20.9 us
    all_to_all x1, starting transfers between devices, sent_and_summed(): parts = lax.all_to_all(in_blocks(array, dim, count), axis, 0, 0, tiled=True)  4.45 us
    unnamed x14, local copies, waits for them, and re-layouts  3.35 us
  transfers between devices with their start and end apart: 3, of which 2 were waited for; matrix products, arithmetic and copies ran while one was open for 6% of the time, Pallas kernels for 0%

commit v1 on v0

v1 whole, which is shorter than its diff:
```python
import jax
import jax.numpy as jnp
import numpy as np
from jax import lax
from jax.experimental import pallas as pl
from jax.experimental.pallas import tpu as pltpu
from jax.sharding import PartitionSpec as P

EPS = 1e-06
SIDE = 8
HALF = SIDE // 2
EVERY = ("rep", "fs", "tp")
OWN = ("fs", "tp")


def place(label, high):
    return 2 * high + (label ^ (high // 2))


QUADS = [
    [place(a, zh) * SIDE + place(b, yh) for a in range(2) for b in range(2)]
    for zh in range(HALF)
    for yh in range(HALF)
]
FAR = [
    [place(a, zh) * SIDE + place(b, yh) for zh in range(HALF) for yh in range(HALF)]
    for a in range(2)
    for b in range(2)
]


def one_row_of_quads():
    order = np.concatenate(
        [
            np.arange(32) + 32 * place(b, yh)
            for b in range(2)
            for yh in range(HALF)
        ]
    )
    return np.eye(256, dtype=np.float32)[:, order]


def nt(left, right):
    return lax.dot_general(
        left, right, (((1,), (1,)), ((), ())), preferred_element_type=jnp.float32
    )


def tn(left, right):
    return lax.dot_general(
        left, right, (((0,), (0,)), ((), ())), preferred_element_type=jnp.float32
    )


def nn(left, right):
    return jnp.dot(left, right, preferred_element_type=jnp.float32)


def local_kernel(near, far, gain, pick, gate_w, up_w, down_w, sent, keep, give, gain_sum):
    xf = jnp.concatenate((near[:, :2048], far[:, :2048]), axis=0).astype(jnp.float32)
    dy = jnp.concatenate((near[:, 2048:], far[:, 2048:]), axis=0)
    inv = lax.rsqrt(jnp.mean(xf * xf, axis=-1, keepdims=True) + EPS)
    normed = xf * inv
    hidden_in = (normed * gain[...]).astype(jnp.bfloat16)
    gate = nt(hidden_in, gate_w[...])
    up = nt(hidden_in, up_w[...])
    sig = 1.0 / (1.0 + jnp.exp(-gate))
    act = gate * sig
    hidden = (act * up).astype(jnp.bfloat16)
    d_hidden = 0.5 * nt(dy, down_w[...])
    d_gate = (d_hidden * up * sig * (1.0 + gate * (1.0 - sig))).astype(jnp.bfloat16)
    d_up = (d_hidden * act).astype(jnp.bfloat16)
    part = nn(d_gate, gate_w[...]) + nn(d_up, up_w[...])
    keep[...] = part[:64]
    give[...] = part[64:].astype(jnp.bfloat16)
    total = jnp.sum(part * normed, axis=0, keepdims=True)
    for k in range(8):
        gain_sum[k : k + 1, :] = total[:, 256 * k : 256 * k + 256]
    for z in range(SIDE):
        zh = z // 2
        a = (z % 2) ^ (zh // 2)
        turned = nn(dy[:, 256 * z : 256 * z + 256], pick[...]).astype(jnp.bfloat16)
        for b in range(2):
            sent[2 * a + b, :128, 128 * zh : 128 * zh + 128] = turned[:, 128 * b : 128 * b + 128]
    for p in range(4):
        sent[p, :128, 512:864] = hidden
        sent[p, :128, 864:] = jnp.zeros((128, 32), jnp.bfloat16)
        sent[p, 128:, :] = jnp.zeros((16, 896), jnp.bfloat16)


def reduce_kernel(got, blocks):
    part = tn(got[0, :128, :512], got[0, :128, 512:])
    for p in range(1, 4):
        part = part + tn(got[p, :128, :512], got[p, :128, 512:])
    part = part.astype(jnp.bfloat16)
    total = jnp.zeros((16, 256), jnp.float32)
    for p in range(4):
        total = total + got[p, 128:, :256].astype(jnp.float32)
    total = total.astype(jnp.bfloat16)
    for k in range(16):
        blocks[k, :32, :] = part[32 * k : 32 * k + 32, :]
        blocks[k, 32:, :256] = total
        blocks[k, 32:, 256:] = jnp.zeros((16, 128), jnp.bfloat16)


def last_kernel(got, down, gain):
    total = got[0].astype(jnp.float32)
    for k in range(1, 16):
        total = total + got[k].astype(jnp.float32)
    down[...] = 0.5 * total[:32, :352]
    for k in range(8):
        gain[:, 256 * k : 256 * k + 256] = total[32 + k : 33 + k, :256]


def call(body, shapes, *args, flops=1000000):
    whole = pl.BlockSpec(memory_space=pltpu.VMEM)
    out = [jax.ShapeDtypeStruct(s, t) for s, t in shapes]
    return pl.pallas_call(
        body,
        out_shape=out,
        in_specs=[whole] * len(args),
        out_specs=[whole] * len(out),
        cost_estimate=pl.CostEstimate(flops=flops, bytes_accessed=4000000, transcendentals=0),
    )(*args)


def to_all(array, axis):
    count = lax.axis_size(axis)
    return lax.all_to_all(
        jnp.broadcast_to(array[None], (count, *array.shape)), axis, 0, 0, tiled=True
    )


def partner(array, axis, bit):
    count = lax.axis_size(axis)
    return lax.ppermute(array, axis, [(i, i ^ bit) for i in range(count)])


def per_device(inputs, cotangent, norm_gain, gate_weight, up_weight, down_weight):
    near = to_all(jnp.concatenate((inputs, cotangent), axis=1), "fs").reshape(64, 4096)
    other = partner(near, "tp", 1)
    pick = jnp.asarray(one_row_of_quads(), jnp.bfloat16)
    sent, keep, give, part_gain = call(
        local_kernel,
        [
            ((4, 144, 896), jnp.bfloat16),
            ((64, 2048), jnp.float32),
            ((64, 2048), jnp.bfloat16),
            ((8, 256), jnp.float32),
        ],
        near,
        other,
        norm_gain.reshape(1, 2048),
        pick,
        gate_weight.T,
        up_weight.T,
        down_weight,
        flops=1000000000,
    )

    group_gain = jnp.sum(to_all(part_gain, OWN).reshape(8, 8, 256), axis=0)
    rows = jnp.broadcast_to(group_gain.astype(jnp.bfloat16)[None], (4, 8, 256))
    sent = lax.dynamic_update_slice(sent, rows, (0, 128, 0))
    got = lax.all_to_all(sent, "rep", 0, 0, tiled=True, axis_index_groups=QUADS)
    (blocks,) = call(reduce_kernel, [((16, 48, 384), jnp.bfloat16)], got)
    got = lax.all_to_all(blocks, "rep", 0, 0, tiled=True, axis_index_groups=FAR)
    down, gain = call(last_kernel, [((32, 352), jnp.float32), ((1, 2048), jnp.float32)], got)
    down_grad = down.T
    gain_grad = gain.reshape(2048)

    chip_in = keep + partner(give, "tp", 1).astype(jnp.float32)
    me = lax.axis_index("fs")
    odd = lax.rem(me, 2)
    pairs = chip_in.reshape(2, 2, 16, 2048)
    mine = lax.dynamic_index_in_dim(pairs, odd, 1, keepdims=False)
    give = lax.dynamic_index_in_dim(pairs, 1 - odd, 1, keepdims=False)
    mine = mine + partner(give.astype(jnp.bfloat16), "fs", 1).astype(jnp.float32)
    high = me // 2
    give = lax.dynamic_index_in_dim(mine, 1 - high, 0, keepdims=False)
    mine = lax.dynamic_index_in_dim(mine, high, 0, keepdims=False)
    d_in = mine + partner(give.astype(jnp.bfloat16), "fs", 2).astype(jnp.float32)

    own_xf = inputs.astype(jnp.float32)
    own_inv = lax.rsqrt(jnp.mean(own_xf * own_xf, axis=-1, keepdims=True) + EPS)
    own_normed = own_xf * own_inv
    scaled = d_in * norm_gain
    input_grad = (
        own_inv * (scaled - own_normed * jnp.mean(scaled * own_normed, axis=-1, keepdims=True))
    ).astype(jnp.bfloat16)
    return (input_grad, gain_grad, down_grad)


def solution(mesh):
    placed = (
        P(EVERY, None),
        P(EVERY, None),
        P(),
        P(None, OWN),
        P(None, OWN),
        P(OWN, None),
    )
    return jax.shard_map(
        per_device,
        mesh=mesh,
        in_specs=placed,
        out_specs=(P(EVERY, None), P(), P(OWN, "rep")),
        check_vma=False,
    )
```

time: 149 us -> 96.3 us (0.65)
  the two profiles are of different devices: /device:TPU:1 before, /device:TPU:64 now
where the time goes in v1:
time: 96.3 us; the launch traced here: 95.6 us
  starting transfers between devices  32 us (33%)
  waiting for transfers between devices  31.7 us (33%)
  blocking collectives  13.6 us (14%)
  Pallas kernels  10.8 us (11%)
  local copies, waits for them, and re-layouts  4.66 us (5%)
  other arithmetic  2.04 us (2%)
    all_to_all x1, blocking collectives, to_all(): lax.all_to_all(jnp.broadcast_to(array[None], (count, *array.shape)), axis...  13.6 us
    all_to_all x1, starting transfers between devices, per_device(): got = lax.all_to_all(blocks, 'rep', 0, 0, tiled=True, axis_index_groups=FAR)  13.5 us
    all_to_all x1, waiting for transfers between devices, per_device(): got = lax.all_to_all(blocks, 'rep', 0, 0, tiled=True, axis_index_groups=FAR)  11.5 us
    pallas_call x3, Pallas kernels, call(): pl.pallas_call(body, out_shape=out, in_specs=[whole] * len(args), out_spe...  10.8 us
    ppermute x4, waiting for transfers between devices, partner(): return lax.ppermute(array, axis, [(i, i ^ bit) for i in range(count)])  10.8 us
    ppermute x4, starting transfers between devices, partner(): return lax.ppermute(array, axis, [(i, i ^ bit) for i in range(count)])  9.61 us
    all_to_all x1, waiting for transfers between devices, per_device(): got = lax.all_to_all(sent, 'rep', 0, 0, tiled=True, axis_index_groups=QUADS)  6.09 us
    all_to_all x1, starting transfers between devices, per_device(): got = lax.all_to_all(sent, 'rep', 0, 0, tiled=True, axis_index_groups=QUADS)  5.52 us
  transfers between devices with their start and end apart: 7, of which 6 were waited for; matrix products, arithmetic and copies ran while one was open for 2% of the time, Pallas kernels for 0%

profile of v1, /device:TPU:64, one launch (start us, length us, event | category | flops | bytes accessed | tf_op | source)
XLA Modules:
  0.0 95.6 jit_solution(1900660733026367479)
XLA Ops:
  0.6 0.9 pad_maximum_fusion
  1.6 13.6 %all_to_all.20 = bf16[4,16,4096]{2,1,0:T(8,128)(2,1)S(1)} all-to-all(bf16[4,16,4096]{2,1,0:T(8,128)(2,1)S(1)} %broadcast_in_dim.6), channel_id=1, replica_groups=mesh['rep'=64,'fs'=4,'tp'=2] {'fs'}, dimensions={0} | all-to-all | bytes 1048576 | tf_op jit(solution)/shard_map/all_to_all | solution.py:129
  15.1 1.9 %collective-permute-start = (bf16[64,4096]{1,0:T(8,128)(2,1)S(1)}, bf16[64,4096]{1,0:T(8,128)(2,1)S(1)}, u32[]{:S(2)}, u32[]{:S(2)}) collective-permute-start(bf16[64,4096]{1,0:T(8,128)(2,1)S(1)} %bitcast.25), channel_id=1, source_target_pairs={{0,1},{1,0},{2,3},{3,2},{4,5},{5,4},{6,7},{7,6},{8,9},{9,8},{10,11... | collective-permute-start | bytes 1572872 | tf_op jit(solution)/shard_map/ppermute | solution.py:136
  17.0 1.9 %collective-permute-done.far = bf16[64,4096]{1,0:T(8,128)(2,1)S(1)} collective-permute-done((bf16[64,4096]{1,0:T(8,128)(2,1)S(1)}, bf16[64,4096]{1,0:T(8,128)(2,1)S(1)}, u32[]{:S(2)}, u32[]{:S(2)}) %collective-permute-start) | collective-permute-done | bytes 524320 | tf_op jit(solution)/shard_map/ppermute | solution.py:136
  18.9 0.8 copy-done.5
  19.7 6.4 %shard_map.94 = (bf16[4,144,896]{2,1,0:T(8,128)(2,1)}, f32[64,2048]{1,0:T(8,128)}, bf16[64,2048]{1,0:T(8,128)(2,1)}, f32[8,256]{1,0:T(8,128)}) custom-call(bf16[64,4096]{1,0:T(8,128)(2,1)} %bitcast.26, bf16[64,4096]{1,0:T(8,128)(2,1)} %copy-done.5, f32[1,2048]{1,0:T(1,128)} %bitcast.31, bf16[256,256]{1,0:T(8,128)(2,1)} %constant.50.clone.pick, ...), custom_call_target="tpu_custom_call" | custom-call | flops 1000000000 | bytes 4000000 | tf_op jit(solution)/shard_map/pallas_call | solution.py:118
  26.2 1.4 %broadcast_in_dim.7 = f32[8,8,256]{2,1,0:T(8,128)} broadcast(f32[8,256]{1,0:T(8,128)} %get-tuple-element.12), dimensions={1,2} | broadcast | bytes 73728 | tf_op jit(solution)/shard_map/broadcast_in_dim | solution.py:130
  27.5 3.4 %all-to-all-start.1 = ((f32[8,8,256]{2,1,0:T(8,128)}), f32[8,8,256]{2,1,0:T(8,128)S(1)}, u32[]{:S(2)}, u32[]{:S(2)}) async-start(f32[8,8,256]{2,1,0:T(8,128)} %broadcast_in_dim.7), calls=%async_computation.1 | async-start | bytes 131072 | tf_op jit(solution)/shard_map/all_to_all | solution.py:129
  30.9 2.3 %collective-permute-start.1 = (bf16[64,2048]{1,0:T(8,128)(2,1)}, bf16[64,2048]{1,0:T(8,128)(2,1)S(1)}, u32[]{:S(2)}, u32[]{:S(2)}) collective-permute-start(bf16[64,2048]{1,0:T(8,128)(2,1)} %get-tuple-element.10), channel_id=1, source_target_pairs={{0,1},{1,0},{2,3},{3,2},{4,5},{5,4},{6,7},{7,6},{8,9},{9,8},{10,11... | collective-permute-start | bytes 786440 | tf_op jit(solution)/shard_map/ppermute | solution.py:136
  33.2 3.2 %all-to-all-done.1 = f32[8,8,256]{2,1,0:T(8,128)S(1)} async-done(((f32[8,8,256]{2,1,0:T(8,128)}), f32[8,8,256]{2,1,0:T(8,128)S(1)}, u32[]{:S(2)}, u32[]{:S(2)}) %all-to-all-start.1) | async-done | bytes 65568 | tf_op jit(solution)/shard_map/all_to_all | solution.py:129
  36.5 0.6 broadcast_dynamic-update-slice_fusion
  37.1 5.5 %all-to-all-start.2 = ((bf16[4,144,896]{2,1,0:T(8,128)(2,1)}), bf16[4,144,896]{2,1,0:T(8,128)(2,1)S(1)}, u32[]{:S(2)}, u32[]{:S(2)}) async-start(bf16[4,144,896]{2,1,0:T(8,128)(2,1)} %broadcast_dynamic-update-slice_fusion), calls=%async_computation.2 | async-start | bytes 2064384 | tf_op jit(solution)/shard_map/all_to_all | solution.py:164
  42.7 2.5 %collective-permute-start.2 = (bf16[2,16,2048]{2,1,0:T(8,128)(2,1)S(1)}, bf16[2,16,2048]{2,1,0:T(8,128)(2,1)S(1)}, u32[]{:S(2)}, u32[]{:S(2)}) collective-permute-start(bf16[2,16,2048]{2,1,0:T(8,128)(2,1)S(1)} %fusion.7), channel_id=1, source_target_pairs={{0,2},{2,0},{4,6},{6,4},{1,3},{3,1},{5,7},{7,5},{8,10},{10,8},{12,... | collective-permute-start | bytes 393224 | tf_op jit(solution)/shard_map/ppermute | solution.py:136
  45.3 4.2 %collective-permute-done.2 = bf16[2,16,2048]{2,1,0:T(8,128)(2,1)S(1)} collective-permute-done((bf16[2,16,2048]{2,1,0:T(8,128)(2,1)S(1)}, bf16[2,16,2048]{2,1,0:T(8,128)(2,1)S(1)}, u32[]{:S(2)}, u32[]{:S(2)}) %collective-permute-start.2) | collective-permute-done | bytes 131104 | tf_op jit(solution)/shard_map/ppermute | solution.py:136
  49.6 6.1 %all-to-all-done.2.got = bf16[4,144,896]{2,1,0:T(8,128)(2,1)S(1)} async-done(((bf16[4,144,896]{2,1,0:T(8,128)(2,1)}), bf16[4,144,896]{2,1,0:T(8,128)(2,1)S(1)}, u32[]{:S(2)}, u32[]{:S(2)}) %all-to-all-start.2) | async-done | bytes 1032224 | tf_op jit(solution)/shard_map/all_to_all | solution.py:164
  55.7 1.0 copy-done
  56.6 2.7 %shard_map.95 = bf16[16,48,384]{2,1,0:T(8,128)(2,1)} custom-call(bf16[4,144,896]{2,1,0:T(8,128)(2,1)} %copy-done), custom_call_target="tpu_custom_call" | custom-call | flops 1000000 | bytes 4000000 | tf_op jit(solution)/shard_map/pallas_call | solution.py:118
  59.3 13.5 %all-to-all-start.3 = ((bf16[16,48,384]{2,1,0:T(8,128)(2,1)}), bf16[16,48,384]{2,1,0:T(8,128)(2,1)S(1)}, u32[]{:S(2)}, u32[]{:S(2)}) async-start(bf16[16,48,384]{2,1,0:T(8,128)(2,1)} %shard_map.95), calls=%async_computation.3 | async-start | bytes 1179648 | tf_op jit(solution)/shard_map/all_to_all | solution.py:166
  72.9 2.9 %collective-permute-start.3 = (bf16[16,2048]{1,0:T(8,128)(2,1)S(1)}, bf16[16,2048]{1,0:T(8,128)(2,1)S(1)}, u32[]{:S(2)}, u32[]{:S(2)}) collective-permute-start(bf16[16,2048]{1,0:T(8,128)(2,1)S(1)} %fusion.9), channel_id=1, source_target_pairs={{0,4},{2,6},{4,0},{6,2},{1,5},{3,7},{5,1},{7,3},{8,12},{10,14},{12... | collective-permute-start | bytes 196616 | tf_op jit(solution)/shard_map/ppermute | solution.py:136
  75.8 4.7 %collective-permute-done.3 = bf16[16,2048]{1,0:T(8,128)(2,1)S(1)} collective-permute-done((bf16[16,2048]{1,0:T(8,128)(2,1)S(1)}, bf16[16,2048]{1,0:T(8,128)(2,1)S(1)}, u32[]{:S(2)}, u32[]{:S(2)}) %collective-permute-start.3) | collective-permute-done | bytes 65568 | tf_op jit(solution)/shard_map/ppermute | solution.py:136
  80.8 0.7 fusion.5
  81.5 11.5 %all-to-all-done.3.got = bf16[16,48,384]{2,1,0:T(8,128)(2,1)S(1)} async-done(((bf16[16,48,384]{2,1,0:T(8,128)(2,1)}), bf16[16,48,384]{2,1,0:T(8,128)(2,1)S(1)}, u32[]{:S(2)}, u32[]{:S(2)}) %all-to-all-start.3) | async-done | bytes 589856 | tf_op jit(solution)/shard_map/all_to_all | solution.py:166
  93.0 0.8 copy-done.1
  93.8 1.7 %shard_map.96 = (f32[32,352]{1,0:T(8,128)}, f32[1,2048]{1,0:T(1,128)}) custom-call(bf16[16,48,384]{2,1,0:T(8,128)(2,1)} %copy-done.1), custom_call_target="tpu_custom_call" | custom-call | flops 1000000 | bytes 4000000 | tf_op jit(solution)/shard_map/pallas_call | solution.py:118
  (22 shorter events, 0.5 us)
Async XLA Ops:
  15.1 3.8 %copy-start.2 = (bf16[4,16,4096]{2,1,0:T(8,128)(2,1)}, bf16[4,16,4096]{2,1,0:T(8,128)(2,1)S(1)}, u32[]{:S(2)}) copy-start(bf16[4,16,4096]{2,1,0:T(8,128)(2,1)S(1)} %all_to_all.20) | copy-start | bytes 1572868
  15.1 3.8 %collective-permute-start = (bf16[64,4096]{1,0:T(8,128)(2,1)S(1)}, bf16[64,4096]{1,0:T(8,128)(2,1)S(1)}, u32[]{:S(2)}, u32[]{:S(2)}) collective-permute-start(bf16[64,4096]{1,0:T(8,128)(2,1)S(1)} %bitcast.25), channel_id=1, source_target_pairs={{0,1},{1,0},{2,3},{3,2},{4,5},{5,4},{6,7},{7,6},{8,9},{9,8},{10,11... | collective-permute-start | bytes 1572872 | tf_op jit(solution)/shard_map/ppermute | solution.py:136
  18.9 0.8 copy-start.5
  26.2 16.4 %copy-start.4 = (f32[64,2048]{1,0:T(8,128)S(1)}, f32[64,2048]{1,0:T(8,128)}, u32[]{:S(2)}) copy-start(f32[64,2048]{1,0:T(8,128)} %get-tuple-element.9) | copy-start | bytes 1572868
  27.5 8.9 %all-to-all-start.1 = ((f32[8,8,256]{2,1,0:T(8,128)}), f32[8,8,256]{2,1,0:T(8,128)S(1)}, u32[]{:S(2)}, u32[]{:S(2)}) async-start(f32[8,8,256]{2,1,0:T(8,128)} %broadcast_in_dim.7), calls=%async_computation.1 | async-start | bytes 131072 | tf_op jit(solution)/shard_map/all_to_all | solution.py:129
  30.9 11.7 %collective-permute-start.1 = (bf16[64,2048]{1,0:T(8,128)(2,1)}, bf16[64,2048]{1,0:T(8,128)(2,1)S(1)}, u32[]{:S(2)}, u32[]{:S(2)}) collective-permute-start(bf16[64,2048]{1,0:T(8,128)(2,1)} %get-tuple-element.10), channel_id=1, source_target_pairs={{0,1},{1,0},{2,3},{3,2},{4,5},{5,4},{6,7},{7,6},{8,9},{9,8},{10,11... | collective-permute-start | bytes 786440 | tf_op jit(solution)/shard_map/ppermute | solution.py:136
  37.1 8.1 %copy-start.3 = (bf16[16,2048]{1,0:T(8,128)(2,1)S(1)}, bf16[16,2048]{1,0:T(8,128)(2,1)}, u32[]{:S(2)}) copy-start(bf16[16,2048]{1,0:T(8,128)(2,1)} %param.7) | copy-start | bytes 196612
  37.1 18.6 %all-to-all-start.2 = ((bf16[4,144,896]{2,1,0:T(8,128)(2,1)}), bf16[4,144,896]{2,1,0:T(8,128)(2,1)S(1)}, u32[]{:S(2)}, u32[]{:S(2)}) async-start(bf16[4,144,896]{2,1,0:T(8,128)(2,1)} %broadcast_dynamic-update-slice_fusion), calls=%async_computation.2 | async-start | bytes 2064384 | tf_op jit(solution)/shard_map/all_to_all | solution.py:164
  42.7 6.9 %collective-permute-start.2 = (bf16[2,16,2048]{2,1,0:T(8,128)(2,1)S(1)}, bf16[2,16,2048]{2,1,0:T(8,128)(2,1)S(1)}, u32[]{:S(2)}, u32[]{:S(2)}) collective-permute-start(bf16[2,16,2048]{2,1,0:T(8,128)(2,1)S(1)} %fusion.7), channel_id=1, source_target_pairs={{0,2},{2,0},{4,6},{6,4},{1,3},{3,1},{5,7},{7,5},{8,10},{10,8},{12,... | collective-permute-start | bytes 393224 | tf_op jit(solution)/shard_map/ppermute | solution.py:136
  49.6 31.0 %copy-start.6 = (f32[2048]{0:T(1024)S(1)}, f32[2048]{0:T(1024)}, u32[]{:S(2)}) copy-start(f32[2048]{0:T(1024)} %param.9) | copy-start | bytes 24580
  55.7 1.0 %copy-start = (bf16[4,144,896]{2,1,0:T(8,128)(2,1)}, bf16[4,144,896]{2,1,0:T(8,128)(2,1)S(1)}, u32[]{:S(2)}) copy-start(bf16[4,144,896]{2,1,0:T(8,128)(2,1)S(1)} %all-to-all-done.2.got) | copy-start | bytes 3096580
  59.3 33.7 %all-to-all-start.3 = ((bf16[16,48,384]{2,1,0:T(8,128)(2,1)}), bf16[16,48,384]{2,1,0:T(8,128)(2,1)S(1)}, u32[]{:S(2)}, u32[]{:S(2)}) async-start(bf16[16,48,384]{2,1,0:T(8,128)(2,1)} %shard_map.95), calls=%async_computation.3 | async-start | bytes 1179648 | tf_op jit(solution)/shard_map/all_to_all | solution.py:166
  72.9 7.7 %collective-permute-start.3 = (bf16[16,2048]{1,0:T(8,128)(2,1)S(1)}, bf16[16,2048]{1,0:T(8,128)(2,1)S(1)}, u32[]{:S(2)}, u32[]{:S(2)}) collective-permute-start(bf16[16,2048]{1,0:T(8,128)(2,1)S(1)} %fusion.9), channel_id=1, source_target_pairs={{0,4},{2,6},{4,0},{6,2},{1,5},{3,7},{5,1},{7,3},{8,12},{10,14},{12... | collective-permute-start | bytes 196616 | tf_op jit(solution)/shard_map/ppermute | solution.py:136
  93.0 0.8 copy-start.1

commit v2 on v1

v2 whole, which is shorter than its diff:
```python
import jax
import jax.numpy as jnp
import numpy as np
from jax import lax
from jax.experimental import pallas as pl
from jax.experimental.pallas import tpu as pltpu
from jax.sharding import PartitionSpec as P


EPS = 1e-06
SIDE = 8
HALF = SIDE // 2
EVERY = ("rep", "fs", "tp")
OWN = ("fs", "tp")


def place(label, high):
    return 2 * high + (label ^ (high // 2))


QUADS = [
    [place(a, zh) * SIDE + place(b, yh) for a in range(2) for b in range(2)]
    for zh in range(HALF)
    for yh in range(HALF)
]
QUAD_DEVICES = [[8 * r + k for r in quad for k in range(8)] for quad in QUADS]
FAR = [
    [place(a, zh) * SIDE + place(b, yh) for zh in range(HALF) for yh in range(HALF)]
    for a in range(2)
    for b in range(2)
]


def one_row_of_quads():
    order = np.concatenate(
        [
            np.arange(32) + 32 * place(b, yh)
            for b in range(2)
            for yh in range(HALF)
        ]
    )
    return np.eye(256, dtype=np.float32)[:, order]


def nt(left, right):
    return lax.dot_general(
        left, right, (((1,), (1,)), ((), ())), preferred_element_type=jnp.float32
    )


def tn(left, right):
    return lax.dot_general(
        left, right, (((0,), (0,)), ((), ())), preferred_element_type=jnp.float32
    )


def nn(left, right):
    return jnp.dot(left, right, preferred_element_type=jnp.float32)


def my_label():
    me = lax.axis_index("rep")
    z, y = me // SIDE, lax.rem(me, SIDE)
    a = lax.rem(z, 2) ^ (z // HALF)
    b = lax.rem(y, 2) ^ (y // HALF)
    return 2 * a + b


def local_kernel(
    near, far, gain, pick, gate_hbm, up_hbm, down_hbm, own, sent_y, sent_z, sent_zy, keep, give,
    gain_sum, turned, gate_w, up_w, down_w, sems,
):
    loads = [
        pltpu.make_async_copy(source, target, sems.at[k])
        for k, (source, target) in enumerate(
            ((gate_hbm, gate_w), (up_hbm, up_w), (down_hbm, down_w))
        )
    ]
    for load in loads:
        load.start()
    xf = jnp.concatenate((near[:, :2048], far[:, :2048]), axis=0).astype(jnp.float32)
    dy = jnp.concatenate((near[:, 2048:], far[:, 2048:]), axis=0)
    inv = lax.rsqrt(jnp.mean(xf * xf, axis=-1, keepdims=True) + EPS)
    normed = xf * inv
    hidden_in = (normed * gain[...]).astype(jnp.bfloat16)
    for z in range(SIDE):
        zh = z // 2
        a = (z % 2) ^ (zh // 2)
        block = nn(dy[:, 256 * z : 256 * z + 256], pick[...]).astype(jnp.bfloat16)
        for b in range(2):
            turned[2 * a + b, :, 128 * zh : 128 * zh + 128] = block[:, 128 * b : 128 * b + 128]
    loads[0].wait()
    gate = nt(hidden_in, gate_w[...])
    loads[1].wait()
    up = nt(hidden_in, up_w[...])
    sig = 1.0 / (1.0 + jnp.exp(-gate))
    act = gate * sig
    hidden = (act * up).astype(jnp.bfloat16)
    loads[2].wait()
    d_hidden = 0.5 * nt(dy, down_w[...])
    d_gate = (d_hidden * up * sig * (1.0 + gate * (1.0 - sig))).astype(jnp.bfloat16)
    d_up = (d_hidden * act).astype(jnp.bfloat16)
    part = nn(d_gate, gate_w[...]) + nn(d_up, up_w[...])
    keep[...] = part[:64]
    give[...] = part[64:].astype(jnp.bfloat16)
    total = jnp.sum(part * normed, axis=0, keepdims=True)
    rows = jnp.concatenate([total[:, 256 * k : 256 * k + 256] for k in range(8)], axis=0)
    for k in range(32):
        gain_sum[k] = rows.astype(jnp.bfloat16)
    mine = my_label()
    for k, out in enumerate((own, sent_y, sent_z, sent_zy)):
        out[:, :512] = turned[mine ^ k]
        out[:, 512:864] = hidden
        out[:, 864:] = jnp.zeros((128, 32), jnp.bfloat16)


def reduce_kernel(own, got_y, got_z, got_zy, gains, blocks):
    part = tn(own[:, :512], own[:, 512:])
    for got in (got_y, got_z, got_zy):
        part = part + tn(got[:, :512], got[:, 512:])
    total = jnp.sum(gains[...].astype(jnp.float32), axis=0).astype(jnp.bfloat16)
    for k in range(16):
        mine = part[32 * k : 32 * k + 32]
        one, two, three, four = (mine[8 * j : 8 * j + 8, 256:352] for j in range(4))
        rest = jnp.concatenate(
            (
                jnp.concatenate((one, two[:, :32]), axis=1),
                jnp.concatenate((two[:, 32:], three[:, :64]), axis=1),
                jnp.concatenate((three[:, 64:], four), axis=1),
            ),
            axis=0,
        )
        blocks[k, :32] = mine[:, :128].astype(jnp.bfloat16)
        blocks[k, 32:64] = mine[:, 128:256].astype(jnp.bfloat16)
        blocks[k, 64:88] = rest.astype(jnp.bfloat16)
        blocks[k, 88:96] = total[:, :128]
        blocks[k, 96:] = total[:, 128:]


def last_kernel(got, down, gain):
    total = got[0].astype(jnp.float32)
    for k in range(1, 16):
        total = total + got[k].astype(jnp.float32)
    one, two, three = (total[64 + 8 * j : 72 + 8 * j] for j in range(3))
    down[:, :128] = 0.5 * total[:32]
    down[:, 128:256] = 0.5 * total[32:64]
    down[:8, 256:] = 0.5 * one[:, :96]
    down[8:16, 256:] = 0.5 * jnp.concatenate((one[:, 96:], two[:, :64]), axis=1)
    down[16:24, 256:] = 0.5 * jnp.concatenate((two[:, 64:], three[:, :32]), axis=1)
    down[24:, 256:] = 0.5 * three[:, 32:]
    for k in range(8):
        for half in range(2):
            at = 256 * k + 128 * half
            gain[:, at : at + 128] = total[88 + 8 * half + k : 89 + 8 * half + k]


def call(body, shapes, *args, scratch=(), flops=1000000, vmem=16, left=0):
    whole = pl.BlockSpec(memory_space=pltpu.VMEM)
    far = pl.BlockSpec(memory_space=pltpu.HBM)
    out = [jax.ShapeDtypeStruct(s, t) for s, t in shapes]
    return pl.pallas_call(
        body,
        out_shape=out,
        in_specs=[whole] * (len(args) - left) + [far] * left,
        out_specs=[whole] * len(out),
        scratch_shapes=scratch,
        cost_estimate=pl.CostEstimate(flops=flops, bytes_accessed=4000000, transcendentals=0),
        compiler_params=pltpu.CompilerParams(vmem_limit_bytes=vmem * 2**20),
    )(*args)


def to_all(array, axis):
    count = lax.axis_size(axis)
    return lax.all_to_all(
        jnp.broadcast_to(array[None], (count, *array.shape)), axis, 0, 0, tiled=True
    )


def partner(array, axis, bit):
    count = lax.axis_size(axis)
    return lax.ppermute(array, axis, [(i, i ^ bit) for i in range(count)])


def per_device(inputs, cotangent, norm_gain, gate_weight, up_weight, down_weight):
    near = to_all(jnp.concatenate((inputs, cotangent), axis=1), "fs").reshape(64, 4096)
    other = partner(near, "tp", 1)
    pick = jnp.asarray(one_row_of_quads(), jnp.bfloat16)
    block = ((128, 896), jnp.bfloat16)
    own, sent_y, sent_z, sent_zy, keep, give, part_gain = call(
        local_kernel,
        [
            block,
            block,
            block,
            block,
            ((64, 2048), jnp.float32),
            ((64, 2048), jnp.bfloat16),
            ((32, 8, 256), jnp.bfloat16),
        ],
        near,
        other,
        norm_gain.reshape(1, 2048),
        pick,
        *(
            pltpu.with_memory_space_constraint(w, pltpu.HBM)
            for w in (gate_weight.T, up_weight.T, down_weight)
        ),
        scratch=[
            pltpu.VMEM((4, 128, 512), jnp.bfloat16),
            pltpu.VMEM((352, 2048), jnp.bfloat16),
            pltpu.VMEM((352, 2048), jnp.bfloat16),
            pltpu.VMEM((352, 2048), jnp.bfloat16),
            pltpu.SemaphoreType.DMA((3,)),
        ],
        flops=1000000000,
        vmem=32,
        left=3,
    )

    gains = lax.all_to_all(
        part_gain, EVERY, 0, 0, tiled=True, axis_index_groups=QUAD_DEVICES
    )
    got_zy = partner(sent_zy, "rep", SIDE + 1)
    got_z = partner(sent_z, "rep", SIDE)
    got_y = partner(sent_y, "rep", 1)
    (blocks,) = call(
        reduce_kernel,
        [((16, 104, 128), jnp.bfloat16)],
        own,
        got_y,
        got_z,
        got_zy,
        gains,
    )
    got = lax.all_to_all(blocks, "rep", 0, 0, tiled=True, axis_index_groups=FAR)
    down, gain = call(last_kernel, [((32, 352), jnp.float32), ((1, 2048), jnp.float32)], got)
    down_grad = down.T
    gain_grad = gain.reshape(2048)

    got = partner(give, "tp", 1)
    chip_in = keep + got.astype(jnp.float32)
    me = lax.axis_index("fs")
    odd = lax.rem(me, 2)
    pairs = chip_in.reshape(2, 2, 16, 2048)
    mine = lax.dynamic_index_in_dim(pairs, odd, 1, keepdims=False)
    give = lax.dynamic_index_in_dim(pairs, 1 - odd, 1, keepdims=False)
    got = partner(give.astype(jnp.bfloat16), "fs", 1)
    mine = mine + got.astype(jnp.float32)
    high = me // 2
    give = lax.dynamic_index_in_dim(mine, 1 - high, 0, keepdims=False)
    mine = lax.dynamic_index_in_dim(mine, high, 0, keepdims=False)
    got = partner(give.astype(jnp.bfloat16), "fs", 2)
    d_in = mine + got.astype(jnp.float32)

    own_xf = inputs.astype(jnp.float32)
    own_inv = lax.rsqrt(jnp.mean(own_xf * own_xf, axis=-1, keepdims=True) + EPS)
    own_normed = own_xf * own_inv
    scaled = d_in * norm_gain
    input_grad = (
        own_inv * (scaled - own_normed * jnp.mean(scaled * own_normed, axis=-1, keepdims=True))
    ).astype(jnp.bfloat16)
    return (input_grad, gain_grad, down_grad)


def solution(mesh):
    placed = (
        P(EVERY, None),
        P(EVERY, None),
        P(),
        P(None, OWN),
        P(None, OWN),
        P(OWN, None),
    )

    return jax.shard_map(
        per_device,
        mesh=mesh,
        in_specs=placed,
        out_specs=(P(EVERY, None), P(), P(OWN, "rep")),
        check_vma=False,
    )
```

time: 96.3 us -> 87 us (0.903)
  the two profiles are of different devices: /device:TPU:64 before, /device:TPU:1 now
where the time goes in v2:
time: 87 us; the launch traced here: 85.7 us
  starting transfers between devices  43.5 us (50%)
  waiting for transfers between devices  20.3 us (23%)
  blocking collectives  11.6 us (13%)
  Pallas kernels  7.24 us (8%)
  other arithmetic  2.08 us (2%)
  between operations  0.87 us (1%)
    ppermute x7, starting transfers between devices, partner(): return lax.ppermute(array, axis, [(i, i ^ bit) for i in range(count)])  25.4 us
    all_to_all x1, waiting for transfers between devices, per_device(): got = lax.all_to_all(blocks, 'rep', 0, 0, tiled=True, axis_index_groups=FAR)  15.4 us
    all_to_all x1, starting transfers between devices, per_device(): got = lax.all_to_all(blocks, 'rep', 0, 0, tiled=True, axis_index_groups=FAR)  12.6 us
    all_to_all x1, blocking collectives, to_all(): lax.all_to_all(jnp.broadcast_to(array[None], (count, *array.shape)), axis...  11.6 us
    pallas_call x3, Pallas kernels, call(): pl.pallas_call(body, out_shape=out, in_specs=[whole] * (len(args) - left)...  7.24 us
    all_to_all x1, starting transfers between devices, per_device(): lax.all_to_all(part_gain, EVERY, 0, 0, tiled=True, axis_index_groups=QUAD...  5.58 us
    ppermute x7, waiting for transfers between devices, partner(): return lax.ppermute(array, axis, [(i, i ^ bit) for i in range(count)])  2.67 us
    all_to_all x1, waiting for transfers between devices, per_device(): lax.all_to_all(part_gain, EVERY, 0, 0, tiled=True, axis_index_groups=QUAD...  2.2 us
  transfers between devices with their start and end apart: 9, of which 4 were waited for; matrix products, arithmetic and copies ran while one was open for 1% of the time, Pallas kernels for 2%

profile of v2, /device:TPU:1, one launch (start us, length us, event | category | flops | bytes accessed | tf_op | source)
XLA Modules:
  0.0 85.7 jit_solution(12216083176846616884)
XLA Ops:
  0.6 0.0 copy-start
  0.7 0.9 %pad_maximum_fusion = bf16[16,4096]{1,0:T(8,128)(2,1)S(1)} fusion(bf16[16,2048]{1,0:T(8,128)(2,1)} %param.8, bf16[16,2048]{1,0:T(8,128)(2,1)} %param.7), kind=kLoop, calls=%fused_computation.13 | loop fusion | flops 262144 | bytes 262144 | tf_op jit(solution)/shard_map/concatenate | solution.py:185
  1.6 11.6 %all_to_all.15 = bf16[4,16,4096]{2,1,0:T(8,128)(2,1)S(1)} all-to-all(bf16[4,16,4096]{2,1,0:T(8,128)(2,1)S(1)} %broadcast_in_dim.2), channel_id=1, replica_groups=mesh['rep'=64,'fs'=4,'tp'=2] {'fs'}, dimensions={0} | all-to-all | bytes 1048576 | tf_op jit(solution)/shard_map/all_to_all | solution.py:174
  13.2 7.7 %collective-permute-start = (bf16[64,4096]{1,0:T(8,128)(2,1)S(1)}, bf16[64,4096]{1,0:T(8,128)(2,1)S(1)}, u32[]{:S(2)}, u32[]{:S(2)}) collective-permute-start(bf16[64,4096]{1,0:T(8,128)(2,1)S(1)} %bitcast.25), channel_id=1, source_target_pairs={{0,1},{1,0},{2,3},{3,2},{4,5},{5,4},{6,7},{7,6},{8,9},{9,8},{10,11... | collective-permute-start | bytes 1572872 | tf_op jit(solution)/shard_map/ppermute | solution.py:181
  20.8 1.5 %collective-permute-done.far = bf16[64,4096]{1,0:T(8,128)(2,1)S(1)} collective-permute-done((bf16[64,4096]{1,0:T(8,128)(2,1)S(1)}, bf16[64,4096]{1,0:T(8,128)(2,1)S(1)}, u32[]{:S(2)}, u32[]{:S(2)}) %collective-permute-start) | collective-permute-done | bytes 524320 | tf_op jit(solution)/shard_map/ppermute | solution.py:181
  22.4 5.1 %shard_map.94 = (bf16[128,896]{1,0:T(8,128)(2,1)S(1)}, bf16[128,896]{1,0:T(8,128)(2,1)S(1)}, bf16[128,896]{1,0:T(8,128)(2,1)S(1)}, bf16[128,896]{1,0:T(8,128)(2,...) custom-call(bf16[64,4096]{1,0:T(8,128)(2,1)S(1)} %bitcast.26, ...), custom_call_target="tpu_custom_call" | custom-call | flops 1000000000 | bytes 4000000 | tf_op jit(solution)/shard_map/pallas_call | solution.py:161
  27.4 0.0 copy-start.2
  27.4 2.4 %collective-permute-start.1 = (bf16[64,2048]{1,0:T(8,128)(2,1)S(1)}, bf16[64,2048]{1,0:T(8,128)(2,1)S(1)}, u32[]{:S(2)}, u32[]{:S(2)}) collective-permute-start(bf16[64,2048]{1,0:T(8,128)(2,1)S(1)} %get-tuple-element.13), channel_id=1, source_target_pairs={{0,1},{1,0},{2,3},{3,2},{4,5},{5,4},{6,7},{7,6},{8,9},{9,8},{10,11... | collective-permute-start | bytes 786440 | tf_op jit(solution)/shard_map/ppermute | solution.py:181
  29.9 1.1 %collective-permute-done.1 = bf16[64,2048]{1,0:T(8,128)(2,1)S(1)} collective-permute-done((bf16[64,2048]{1,0:T(8,128)(2,1)S(1)}, bf16[64,2048]{1,0:T(8,128)(2,1)S(1)}, u32[]{:S(2)}, u32[]{:S(2)}) %collective-permute-start.1) | collective-permute-done | bytes 262176 | tf_op jit(solution)/shard_map/ppermute | solution.py:181
  31.0 0.1 convert_add_fusion
  31.1 2.2 %collective-permute-start.2 = (bf16[2,16,2048]{2,1,0:T(8,128)(2,1)S(1)}, bf16[2,16,2048]{2,1,0:T(8,128)(2,1)S(1)}, u32[]{:S(2)}, u32[]{:S(2)}) collective-permute-start(bf16[2,16,2048]{2,1,0:T(8,128)(2,1)S(1)} %fusion.7), channel_id=1, source_target_pairs={{0,2},{2,0},{4,6},{6,4},{1,3},{3,1},{5,7},{7,5},{8,10},{10,8},{12,... | collective-permute-start | bytes 393224 | tf_op jit(solution)/shard_map/ppermute | solution.py:181
  33.3 0.1 fusion.6
  33.5 1.9 %collective-permute-start.4 = (bf16[128,896]{1,0:T(8,128)(2,1)S(1)}, bf16[128,896]{1,0:T(8,128)(2,1)S(1)}, u32[]{:S(2)}, u32[]{:S(2)}) collective-permute-start(bf16[128,896]{1,0:T(8,128)(2,1)S(1)} %get-tuple-element.15), channel_id=1, source_target_pairs={{0,8},{8,0},{16,24},{24,16},{32,40},{40,32},{48,56},{56,48},{64,72... | collective-permute-start | bytes 688136 | tf_op jit(solution)/shard_map/ppermute | solution.py:181
  35.4 3.0 %collective-permute-start.5 = (bf16[128,896]{1,0:T(8,128)(2,1)S(1)}, bf16[128,896]{1,0:T(8,128)(2,1)S(1)}, u32[]{:S(2)}, u32[]{:S(2)}) collective-permute-start(bf16[128,896]{1,0:T(8,128)(2,1)S(1)} %get-tuple-element.16), channel_id=1, source_target_pairs={{0,64},{8,72},{16,80},{24,88},{32,96},{40,104},{48,112},{56,120},{... | collective-permute-start | bytes 688136 | tf_op jit(solution)/shard_map/ppermute | solution.py:181
  38.4 3.4 %collective-permute-start.6 = (bf16[128,896]{1,0:T(8,128)(2,1)S(1)}, bf16[128,896]{1,0:T(8,128)(2,1)S(1)}, u32[]{:S(2)}, u32[]{:S(2)}) collective-permute-start(bf16[128,896]{1,0:T(8,128)(2,1)S(1)} %get-tuple-element.17), channel_id=1, source_target_pairs={{0,72},{8,64},{16,88},{24,80},{32,104},{40,96},{48,120},{56,112},{... | collective-permute-start | bytes 688136 | tf_op jit(solution)/shard_map/ppermute | solution.py:181
  41.9 5.6 %all-to-all-start.1 = ((bf16[32,8,256]{2,1,0:T(8,128)(2,1)}), bf16[32,8,256]{2,1,0:T(8,128)(2,1)S(1)}, u32[]{:S(2)}, u32[]{:S(2)}) async-start(bf16[32,8,256]{2,1,0:T(8,128)(2,1)} %get-tuple-element.18), calls=%async_computation.1 | async-start | bytes 262144 | tf_op jit(solution)/shard_map/all_to_all | solution.py:220
  47.5 4.8 %collective-permute-start.3 = (bf16[16,2048]{1,0:T(8,128)(2,1)S(1)}, bf16[16,2048]{1,0:T(8,128)(2,1)S(1)}, u32[]{:S(2)}, u32[]{:S(2)}) collective-permute-start(bf16[16,2048]{1,0:T(8,128)(2,1)S(1)} %fusion.9), channel_id=1, source_target_pairs={{0,4},{2,6},{4,0},{6,2},{1,5},{3,7},{5,1},{7,3},{8,12},{10,14},{12... | collective-permute-start | bytes 196616 | tf_op jit(solution)/shard_map/ppermute | solution.py:181
  52.3 2.2 %all-to-all-done.1.gains = bf16[32,8,256]{2,1,0:T(8,128)(2,1)S(1)} async-done(((bf16[32,8,256]{2,1,0:T(8,128)(2,1)}), bf16[32,8,256]{2,1,0:T(8,128)(2,1)S(1)}, u32[]{:S(2)}, u32[]{:S(2)}) %all-to-all-start.1) | async-done | bytes 131104 | tf_op jit(solution)/shard_map/all_to_all | solution.py:220
  54.5 1.4 %shard_map.95 = bf16[16,104,128]{2,1,0:T(8,128)(2,1)} custom-call(bf16[128,896]{1,0:T(8,128)(2,1)S(1)} %get-tuple-element.14.own, bf16[128,896]{1,0:T(8,128)(2,1)S(1)} %collective-permute-done.4.got_y, bf16[128,896]{1,0:T(8,128)(2,1)S(1)} %collective-permute-done.5.got_z, bf16[128,896]{1,0:T(8,128)(2,1)S(1)} %collective-permute-done.6.got_zy, ...), custom_call_target="tpu_custom_call" | custom-call | flops 1000000 | bytes 4000000 | tf_op jit(solution)/shard_map/pallas_call | solution.py:161
  56.0 12.6 %all-to-all-start.2 = ((bf16[16,104,128]{2,1,0:T(8,128)(2,1)}), bf16[16,104,128]{2,1,0:T(8,128)(2,1)S(1)}, u32[]{:S(2)}, u32[]{:S(2)}) async-start(bf16[16,104,128]{2,1,0:T(8,128)(2,1)} %shard_map.95), calls=%async_computation.2 | async-start | bytes 851968 | tf_op jit(solution)/shard_map/all_to_all | solution.py:235
  68.5 0.2 fusion.2
  68.7 0.7 fusion.5
  69.5 15.4 %all-to-all-done.2.got = bf16[16,104,128]{2,1,0:T(8,128)(2,1)S(1)} async-done(((bf16[16,104,128]{2,1,0:T(8,128)(2,1)}), bf16[16,104,128]{2,1,0:T(8,128)(2,1)S(1)}, u32[]{:S(2)}, u32[]{:S(2)}) %all-to-all-start.2) | async-done | bytes 426016 | tf_op jit(solution)/shard_map/all_to_all | solution.py:235
  84.9 0.8 shard_map.96
  (15 shorter events, 0.1 us)
Async XLA Ops:
  0.6 21.7 %copy-start = (bf16[256,256]{1,0:T(8,128)(2,1)S(1)}, bf16[256,256]{1,0:T(8,128)(2,1)}, u32[]{:S(2)}) copy-start(bf16[256,256]{1,0:T(8,128)(2,1)} %constant.47.clone.pick) | copy-start | bytes 393220
  0.6 21.7 %copy-start.1 = (f32[2048]{0:T(1024)S(1)}, f32[2048]{0:T(1024)}, u32[]{:S(2)}) copy-start(f32[2048]{0:T(1024)} %param.9) | copy-start | bytes 24580
  13.2 9.2 %collective-permute-start = (bf16[64,4096]{1,0:T(8,128)(2,1)S(1)}, bf16[64,4096]{1,0:T(8,128)(2,1)S(1)}, u32[]{:S(2)}, u32[]{:S(2)}) collective-permute-start(bf16[64,4096]{1,0:T(8,128)(2,1)S(1)} %bitcast.25), channel_id=1, source_target_pairs={{0,1},{1,0},{2,3},{3,2},{4,5},{5,4},{6,7},{7,6},{8,9},{9,8},{10,11... | collective-permute-start | bytes 1572872 | tf_op jit(solution)/shard_map/ppermute | solution.py:181
  27.4 5.9 %copy-start.2 = (bf16[16,2048]{1,0:T(8,128)(2,1)S(1)}, bf16[16,2048]{1,0:T(8,128)(2,1)}, u32[]{:S(2)}) copy-start(bf16[16,2048]{1,0:T(8,128)(2,1)} %param.7) | copy-start | bytes 196612
  27.4 3.6 %collective-permute-start.1 = (bf16[64,2048]{1,0:T(8,128)(2,1)S(1)}, bf16[64,2048]{1,0:T(8,128)(2,1)S(1)}, u32[]{:S(2)}, u32[]{:S(2)}) collective-permute-start(bf16[64,2048]{1,0:T(8,128)(2,1)S(1)} %get-tuple-element.13), channel_id=1, source_target_pairs={{0,1},{1,0},{2,3},{3,2},{4,5},{5,4},{6,7},{7,6},{8,9},{9,8},{10,11... | collective-permute-start | bytes 786440 | tf_op jit(solution)/shard_map/ppermute | solution.py:181
  31.1 16.3 %collective-permute-start.2 = (bf16[2,16,2048]{2,1,0:T(8,128)(2,1)S(1)}, bf16[2,16,2048]{2,1,0:T(8,128)(2,1)S(1)}, u32[]{:S(2)}, u32[]{:S(2)}) collective-permute-start(bf16[2,16,2048]{2,1,0:T(8,128)(2,1)S(1)} %fusion.7), channel_id=1, source_target_pairs={{0,2},{2,0},{4,6},{6,4},{1,3},{3,1},{5,7},{7,5},{8,10},{10,8},{12,... | collective-permute-start | bytes 393224 | tf_op jit(solution)/shard_map/ppermute | solution.py:181
  33.5 18.8 %collective-permute-start.4 = (bf16[128,896]{1,0:T(8,128)(2,1)S(1)}, bf16[128,896]{1,0:T(8,128)(2,1)S(1)}, u32[]{:S(2)}, u32[]{:S(2)}) collective-permute-start(bf16[128,896]{1,0:T(8,128)(2,1)S(1)} %get-tuple-element.15), channel_id=1, source_target_pairs={{0,8},{8,0},{16,24},{24,16},{32,40},{40,32},{48,56},{56,48},{64,72... | collective-permute-start | bytes 688136 | tf_op jit(solution)/shard_map/ppermute | solution.py:181
  35.4 16.9 %collective-permute-start.5 = (bf16[128,896]{1,0:T(8,128)(2,1)S(1)}, bf16[128,896]{1,0:T(8,128)(2,1)S(1)}, u32[]{:S(2)}, u32[]{:S(2)}) collective-permute-start(bf16[128,896]{1,0:T(8,128)(2,1)S(1)} %get-tuple-element.16), channel_id=1, source_target_pairs={{0,64},{8,72},{16,80},{24,88},{32,96},{40,104},{48,112},{56,120},{... | collective-permute-start | bytes 688136 | tf_op jit(solution)/shard_map/ppermute | solution.py:181
  38.4 13.9 %collective-permute-start.6 = (bf16[128,896]{1,0:T(8,128)(2,1)S(1)}, bf16[128,896]{1,0:T(8,128)(2,1)S(1)}, u32[]{:S(2)}, u32[]{:S(2)}) collective-permute-start(bf16[128,896]{1,0:T(8,128)(2,1)S(1)} %get-tuple-element.17), channel_id=1, source_target_pairs={{0,72},{8,64},{16,88},{24,80},{32,104},{40,96},{48,120},{56,112},{... | collective-permute-start | bytes 688136 | tf_op jit(solution)/shard_map/ppermute | solution.py:181
  41.9 12.7 %all-to-all-start.1 = ((bf16[32,8,256]{2,1,0:T(8,128)(2,1)}), bf16[32,8,256]{2,1,0:T(8,128)(2,1)S(1)}, u32[]{:S(2)}, u32[]{:S(2)}) async-start(bf16[32,8,256]{2,1,0:T(8,128)(2,1)} %get-tuple-element.18), calls=%async_computation.1 | async-start | bytes 262144 | tf_op jit(solution)/shard_map/all_to_all | solution.py:220
  47.5 21.0 %collective-permute-start.3 = (bf16[16,2048]{1,0:T(8,128)(2,1)S(1)}, bf16[16,2048]{1,0:T(8,128)(2,1)S(1)}, u32[]{:S(2)}, u32[]{:S(2)}) collective-permute-start(bf16[16,2048]{1,0:T(8,128)(2,1)S(1)} %fusion.9), channel_id=1, source_target_pairs={{0,4},{2,6},{4,0},{6,2},{1,5},{3,7},{5,1},{7,3},{8,12},{10,14},{12... | collective-permute-start | bytes 196616 | tf_op jit(solution)/shard_map/ppermute | solution.py:181
  56.0 28.9 %all-to-all-start.2 = ((bf16[16,104,128]{2,1,0:T(8,128)(2,1)}), bf16[16,104,128]{2,1,0:T(8,128)(2,1)S(1)}, u32[]{:S(2)}, u32[]{:S(2)}) async-start(bf16[16,104,128]{2,1,0:T(8,128)(2,1)} %shard_map.95), calls=%async_computation.2 | async-start | bytes 851968 | tf_op jit(solution)/shard_map/all_to_all | solution.py:235

commit v3 on v2

--- a/solution.py
+++ b/solution.py
@@ -67,17 +67,22 @@
 
 
 def local_kernel(
-    near, far, gain, pick, gate_hbm, up_hbm, down_hbm, own, sent_y, sent_z, sent_zy, keep, give,
-    gain_sum, turned, gate_w, up_w, down_w, sems,
+    near, far, gain, pick, gate_w, up_hbm, down_hbm, own, sent_y, sent_z, sent_zy, keep, give,
+    gain_sum, turned, up_w, down_w, gain_rows, sems,
 ):
     loads = [
         pltpu.make_async_copy(source, target, sems.at[k])
-        for k, (source, target) in enumerate(
-            ((gate_hbm, gate_w), (up_hbm, up_w), (down_hbm, down_w))
-        )
+        for k, (source, target) in enumerate(((up_hbm, up_w), (down_hbm, down_w)))
     ]
-    for load in loads:
-        load.start()
+    mine = my_label()
+
+    once = jnp.minimum(mine, 0) + 1
+
+    @pl.loop(0, once)
+    def _(_):
+        for load in loads:
+            load.start()
+
     xf = jnp.concatenate((near[:, :2048], far[:, :2048]), axis=0).astype(jnp.float32)
     dy = jnp.concatenate((near[:, 2048:], far[:, 2048:]), axis=0)
     inv = lax.rsqrt(jnp.mean(xf * xf, axis=-1, keepdims=True) + EPS)
@@ -89,14 +94,13 @@
         block = nn(dy[:, 256 * z : 256 * z + 256], pick[...]).astype(jnp.bfloat16)
         for b in range(2):
             turned[2 * a + b, :, 128 * zh : 128 * zh + 128] = block[:, 128 * b : 128 * b + 128]
+    gate = nt(hidden_in, gate_w[...])
     loads[0].wait()
-    gate = nt(hidden_in, gate_w[...])
-    loads[1].wait()
     up = nt(hidden_in, up_w[...])
     sig = 1.0 / (1.0 + jnp.exp(-gate))
     act = gate * sig
     hidden = (act * up).astype(jnp.bfloat16)
-    loads[2].wait()
+    loads[1].wait()
     d_hidden = 0.5 * nt(dy, down_w[...])
     d_gate = (d_hidden * up * sig * (1.0 + gate * (1.0 - sig))).astype(jnp.bfloat16)
     d_up = (d_hidden * act).astype(jnp.bfloat16)
@@ -106,12 +110,18 @@
     total = jnp.sum(part * normed, axis=0, keepdims=True)
     rows = jnp.concatenate([total[:, 256 * k : 256 * k + 256] for k in range(8)], axis=0)
     for k in range(32):
-        gain_sum[k] = rows.astype(jnp.bfloat16)
-    mine = my_label()
+        gain_rows[k] = rows.astype(jnp.bfloat16)
+    store = pltpu.make_async_copy(gain_rows, gain_sum, sems.at[2])
+
+    @pl.loop(0, once)
+    def _(_):
+        store.start()
+
     for k, out in enumerate((own, sent_y, sent_z, sent_zy)):
         out[:, :512] = turned[mine ^ k]
         out[:, 512:864] = hidden
         out[:, 864:] = jnp.zeros((128, 32), jnp.bfloat16)
+    store.wait()
 
 
 def reduce_kernel(own, got_y, got_z, got_zy, gains, blocks):
@@ -154,7 +164,26 @@
             gain[:, at : at + 128] = total[88 + 8 * half + k : 89 + 8 * half + k]
 
 
-def call(body, shapes, *args, scratch=(), flops=1000000, vmem=16, left=0):
+def split_kernel(keep, got, mine, to_one, to_two, to_three):
+    me = lax.axis_index("fs")
+    for k, out in enumerate((mine, to_one, to_two, to_three)):
+        rows = pl.ds(pl.multiple_of(16 * (me ^ k), 16), 16)
+        out[...] = (keep[rows, :] + got[rows, :].astype(jnp.float32)).astype(out.dtype)
+
+
+def input_kernel(mine, from_one, from_two, from_three, inputs, gain, out):
+    d_in = mine[...]
+    for got in (from_one, from_two, from_three):
+        d_in = d_in + got[...].astype(jnp.float32)
+    xf = inputs[...].astype(jnp.float32)
+    inv = lax.rsqrt(jnp.mean(xf * xf, axis=-1, keepdims=True) + EPS)
+    normed = xf * inv
+    scaled = d_in * gain[...]
+    mean = jnp.mean(scaled * normed, axis=-1, keepdims=True)
+    out[...] = (inv * (scaled - normed * mean)).astype(out.dtype)
+
+
+def call(body, shapes, *args, scratch=(), flops=1000000, vmem=16, left=0, last=0):
     whole = pl.BlockSpec(memory_space=pltpu.VMEM)
     far = pl.BlockSpec(memory_space=pltpu.HBM)
     out = [jax.ShapeDtypeStruct(s, t) for s, t in shapes]
@@ -162,7 +191,7 @@
         body,
         out_shape=out,
         in_specs=[whole] * (len(args) - left) + [far] * left,
-        out_specs=[whole] * len(out),
+        out_specs=[whole] * (len(out) - last) + [far] * last,
         scratch_shapes=scratch,
         cost_estimate=pl.CostEstimate(flops=flops, bytes_accessed=4000000, transcendentals=0),
         compiler_params=pltpu.CompilerParams(vmem_limit_bytes=vmem * 2**20),
@@ -201,20 +230,20 @@
         other,
         norm_gain.reshape(1, 2048),
         pick,
-        *(
-            pltpu.with_memory_space_constraint(w, pltpu.HBM)
-            for w in (gate_weight.T, up_weight.T, down_weight)
-        ),
+        gate_weight.T,
+        pltpu.with_memory_space_constraint(up_weight.T, pltpu.HBM),
+        pltpu.with_memory_space_constraint(down_weight, pltpu.HBM),
         scratch=[
             pltpu.VMEM((4, 128, 512), jnp.bfloat16),
             pltpu.VMEM((352, 2048), jnp.bfloat16),
             pltpu.VMEM((352, 2048), jnp.bfloat16),
-            pltpu.VMEM((352, 2048), jnp.bfloat16),
+            pltpu.VMEM((32, 8, 256), jnp.bfloat16),
             pltpu.SemaphoreType.DMA((3,)),
         ],
         flops=1000000000,
         vmem=32,
-        left=3,
+        left=2,
+        last=1,
     )
 
     gains = lax.all_to_all(
@@ -238,27 +267,16 @@
     gain_grad = gain.reshape(2048)
 
     got = partner(give, "tp", 1)
-    chip_in = keep + got.astype(jnp.float32)
-    me = lax.axis_index("fs")
-    odd = lax.rem(me, 2)
-    pairs = chip_in.reshape(2, 2, 16, 2048)
-    mine = lax.dynamic_index_in_dim(pairs, odd, 1, keepdims=False)
-    give = lax.dynamic_index_in_dim(pairs, 1 - odd, 1, keepdims=False)
-    got = partner(give.astype(jnp.bfloat16), "fs", 1)
-    mine = mine + got.astype(jnp.float32)
-    high = me // 2
-    give = lax.dynamic_index_in_dim(mine, 1 - high, 0, keepdims=False)
-    mine = lax.dynamic_index_in_dim(mine, high, 0, keepdims=False)
-    got = partner(give.astype(jnp.bfloat16), "fs", 2)
-    d_in = mine + got.astype(jnp.float32)
-
-    own_xf = inputs.astype(jnp.float32)
-    own_inv = lax.rsqrt(jnp.mean(own_xf * own_xf, axis=-1, keepdims=True) + EPS)
-    own_normed = own_xf * own_inv
-    scaled = d_in * norm_gain
-    input_grad = (
-        own_inv * (scaled - own_normed * jnp.mean(scaled * own_normed, axis=-1, keepdims=True))
-    ).astype(jnp.bfloat16)
+    tokens = ((16, 2048), jnp.bfloat16)
+    mine, *sends = call(
+        split_kernel, [((16, 2048), jnp.float32), tokens, tokens, tokens], keep, got
+    )
+    gots = []
+    for k in range(3):
+        gots.append(partner(sends[k], "fs", k + 1))
+    (input_grad,) = call(
+        input_kernel, [tokens], mine, *gots, inputs, norm_gain.reshape(1, 2048)
+    )
     return (input_grad, gain_grad, down_grad)
 
 

time: 87 us -> 82.8 us (0.952)
  waiting for transfers between devices: 20.3 us -> 13.9 us
  starting transfers between devices: 43.5 us -> 46.7 us
  other arithmetic: 2.08 us -> 1 us
    all_to_all x1, waiting for transfers between devices: 15.4 us -> 0.01 us  [per_device(): got = lax.all_to_all(blocks, 'rep', 0, 0, tiled=True, axis_index_groups=FAR)]
    ppermute x7 -> x8, waiting for transfers between devices: 2.67 us -> 13.9 us  [partner(): return lax.ppermute(array, axis, [(i, i ^ bit) for i in range(count)])]
    ppermute x7 -> x8, starting transfers between devices: 25.4 us -> 30.4 us  [partner(): return lax.ppermute(array, axis, [(i, i ^ bit) for i in range(count)])]
    all_to_all x1, waiting for transfers between devices: 2.2 us -> 0.01 us  [per_device(): lax.all_to_all(part_gain, EVERY, 0, 0, tiled=True, axis_index_groups=QUAD...]
    all_to_all x1, starting transfers between devices: 5.58 us -> 3.93 us  [per_device(): lax.all_to_all(part_gain, EVERY, 0, 0, tiled=True, axis_index_groups=QUAD...]
    pallas_call x3 -> x5, Pallas kernels: 7.24 us -> 7.42 us  [call(): pl.pallas_call(body, out_shape=out, in_specs=[whole] * (len(args) - left)...]
  transfers between devices with their start and end apart: 9 -> 10, of which waited for: 4 -> 7; matrix products, arithmetic and copies ran while one was open for 1% -> 0% of each run, Pallas kernels for 2% -> 1%
where the time goes in v3:
time: 82.8 us; the launch traced here: 81.4 us
  starting transfers between devices  46.7 us (56%)
  waiting for transfers between devices  13.9 us (17%)
  blocking collectives  11.6 us (14%)
  Pallas kernels  7.42 us (9%)
  other arithmetic  1 us (1%)
    ppermute x8, starting transfers between devices, partner(): return lax.ppermute(array, axis, [(i, i ^ bit) for i in range(count)])  30.4 us
    ppermute x8, waiting for transfers between devices, partner(): return lax.ppermute(array, axis, [(i, i ^ bit) for i in range(count)])  13.9 us
    all_to_all x1, starting transfers between devices, per_device(): got = lax.all_to_all(blocks, 'rep', 0, 0, tiled=True, axis_index_groups=FAR)  12.4 us
    all_to_all x1, blocking collectives, to_all(): lax.all_to_all(jnp.broadcast_to(array[None], (count, *array.shape)), axis...  11.6 us
    pallas_call x5, Pallas kernels, call(): pl.pallas_call(body, out_shape=out, in_specs=[whole] * (len(args) - left)...  7.42 us
    all_to_all x1, starting transfers between devices, per_device(): lax.all_to_all(part_gain, EVERY, 0, 0, tiled=True, axis_index_groups=QUAD...  3.93 us
  transfers between devices with their start and end apart: 10, of which 7 were waited for; matrix products, arithmetic and copies ran while one was open for 0% of the time, Pallas kernels for 1%

profile of v3, /device:TPU:1, one launch (start us, length us, event | category | flops | bytes accessed | tf_op | source)
XLA Modules:
  0.0 81.4 jit_solution(17295128852553769721)
XLA Ops:
  0.6 0.0 copy-start.2
  0.7 1.0 %pad_maximum_fusion = bf16[16,4096]{1,0:T(8,128)(2,1)S(1)} fusion(bf16[16,2048]{1,0:T(8,128)(2,1)} %param.8, bf16[16,2048]{1,0:T(8,128)(2,1)} %inputs.1), kind=kLoop, calls=%fused_computation | loop fusion | flops 262144 | bytes 262144 | tf_op jit(solution)/shard_map/concatenate | solution.py:214
  1.7 11.6 %all_to_all.15 = bf16[4,16,4096]{2,1,0:T(8,128)(2,1)S(1)} all-to-all(bf16[4,16,4096]{2,1,0:T(8,128)(2,1)S(1)} %broadcast_in_dim.2), channel_id=1, replica_groups=mesh['rep'=64,'fs'=4,'tp'=2] {'fs'}, dimensions={0} | all-to-all | bytes 1048576 | tf_op jit(solution)/shard_map/all_to_all | solution.py:203
  13.3 7.7 %collective-permute-start = (bf16[64,4096]{1,0:T(8,128)(2,1)S(1)}, bf16[64,4096]{1,0:T(8,128)(2,1)S(1)}, u32[]{:S(2)}, u32[]{:S(2)}) collective-permute-start(bf16[64,4096]{1,0:T(8,128)(2,1)S(1)} %bitcast.6), channel_id=1, source_target_pairs={{0,1},{1,0},{2,3},{3,2},{4,5},{5,4},{6,7},{7,6},{8,9},{9,8},{10,11... | collective-permute-start | bytes 1572872 | tf_op jit(solution)/shard_map/ppermute | solution.py:210
  20.9 1.5 %collective-permute-done.far = bf16[64,4096]{1,0:T(8,128)(2,1)S(1)} collective-permute-done((bf16[64,4096]{1,0:T(8,128)(2,1)S(1)}, bf16[64,4096]{1,0:T(8,128)(2,1)S(1)}, u32[]{:S(2)}, u32[]{:S(2)}) %collective-permute-start) | collective-permute-done | bytes 524320 | tf_op jit(solution)/shard_map/ppermute | solution.py:210
  22.5 4.3 %shard_map.94 = (bf16[128,896]{1,0:T(8,128)(2,1)S(1)}, bf16[128,896]{1,0:T(8,128)(2,1)S(1)}, bf16[128,896]{1,0:T(8,128)(2,1)S(1)}, bf16[128,896]{1,0:T(8,128)(2,...) custom-call(bf16[64,4096]{1,0:T(8,128)(2,1)S(1)} %bitcast.7, ...), custom_call_target="tpu_custom_call" | custom-call | flops 1000000000 | bytes 4000000 | tf_op jit(solution)/shard_map/pallas_call | solution.py:190
  26.8 3.9 %all-to-all-start.1 = ((bf16[32,8,256]{2,1,0:T(8,128)(2,1)}), bf16[32,8,256]{2,1,0:T(8,128)(2,1)S(1)}, u32[]{:S(2)}, u32[]{:S(2)}) async-start(bf16[32,8,256]{2,1,0:T(8,128)(2,1)} %get-tuple-element.26), calls=%async_computation.1 | async-start | bytes 262144 | tf_op jit(solution)/shard_map/all_to_all | solution.py:249
  30.7 3.3 %collective-permute-start.5 = (bf16[128,896]{1,0:T(8,128)(2,1)S(1)}, bf16[128,896]{1,0:T(8,128)(2,1)S(1)}, u32[]{:S(2)}, u32[]{:S(2)}) collective-permute-start(bf16[128,896]{1,0:T(8,128)(2,1)S(1)} %get-tuple-element.23), channel_id=1, source_target_pairs={{0,8},{8,0},{16,24},{24,16},{32,40},{40,32},{48,56},{56,48},{64,72... | collective-permute-start | bytes 688136 | tf_op jit(solution)/shard_map/ppermute | solution.py:210
  34.1 3.2 %collective-permute-start.6 = (bf16[128,896]{1,0:T(8,128)(2,1)S(1)}, bf16[128,896]{1,0:T(8,128)(2,1)S(1)}, u32[]{:S(2)}, u32[]{:S(2)}) collective-permute-start(bf16[128,896]{1,0:T(8,128)(2,1)S(1)} %get-tuple-element.24), channel_id=1, source_target_pairs={{0,64},{8,72},{16,80},{24,88},{32,96},{40,104},{48,112},{56,120},{... | collective-permute-start | bytes 688136 | tf_op jit(solution)/shard_map/ppermute | solution.py:210
  37.3 1.9 %collective-permute-start.7 = (bf16[128,896]{1,0:T(8,128)(2,1)S(1)}, bf16[128,896]{1,0:T(8,128)(2,1)S(1)}, u32[]{:S(2)}, u32[]{:S(2)}) collective-permute-start(bf16[128,896]{1,0:T(8,128)(2,1)S(1)} %get-tuple-element.25), channel_id=1, source_target_pairs={{0,72},{8,64},{16,88},{24,80},{32,104},{40,96},{48,120},{56,112},{... | collective-permute-start | bytes 688136 | tf_op jit(solution)/shard_map/ppermute | solution.py:210
  39.2 0.2 collective-permute-done.5.got_y
  39.4 6.9 %collective-permute-done.6.got_z = bf16[128,896]{1,0:T(8,128)(2,1)S(1)} collective-permute-done((bf16[128,896]{1,0:T(8,128)(2,1)S(1)}, bf16[128,896]{1,0:T(8,128)(2,1)S(1)}, u32[]{:S(2)}, u32[]{:S(2)}) %collective-permute-start.6) | collective-permute-done | bytes 229408 | tf_op jit(solution)/shard_map/ppermute | solution.py:210
  46.3 0.1 collective-permute-done.7.got_zy
  46.4 1.4 %shard_map.97 = bf16[16,104,128]{2,1,0:T(8,128)(2,1)} custom-call(bf16[128,896]{1,0:T(8,128)(2,1)S(1)} %get-tuple-element.22.own, bf16[128,896]{1,0:T(8,128)(2,1)S(1)} %collective-permute-done.5.got_y, bf16[128,896]{1,0:T(8,128)(2,1)S(1)} %collective-permute-done.6.got_z, bf16[128,896]{1,0:T(8,128)(2,1)S(1)} %collective-permute-done.7.got_zy, ...), custom_call_target="tpu_custom_call" | custom-call | flops 1000000 | bytes 4000000 | tf_op jit(solution)/shard_map/pallas_call | solution.py:190
  47.8 12.4 %all-to-all-start.2 = ((bf16[16,104,128]{2,1,0:T(8,128)(2,1)}), bf16[16,104,128]{2,1,0:T(8,128)(2,1)S(1)}, u32[]{:S(2)}, u32[]{:S(2)}) async-start(bf16[16,104,128]{2,1,0:T(8,128)(2,1)} %shard_map.97), calls=%async_computation.2 | async-start | bytes 851968 | tf_op jit(solution)/shard_map/all_to_all | solution.py:264
  60.2 4.7 %collective-permute-start.1 = (bf16[64,2048]{1,0:T(8,128)(2,1)S(1)}, bf16[64,2048]{1,0:T(8,128)(2,1)S(1)}, u32[]{:S(2)}, u32[]{:S(2)}) collective-permute-start(bf16[64,2048]{1,0:T(8,128)(2,1)S(1)} %get-tuple-element.17), channel_id=1, source_target_pairs={{0,1},{1,0},{2,3},{3,2},{4,5},{5,4},{6,7},{7,6},{8,9},{9,8},{10,11... | collective-permute-start | bytes 786440 | tf_op jit(solution)/shard_map/ppermute | solution.py:210
  64.9 1.1 %collective-permute-done.1.got = bf16[64,2048]{1,0:T(8,128)(2,1)S(1)} collective-permute-done((bf16[64,2048]{1,0:T(8,128)(2,1)S(1)}, bf16[64,2048]{1,0:T(8,128)(2,1)S(1)}, u32[]{:S(2)}, u32[]{:S(2)}) %collective-permute-start.1) | collective-permute-done | bytes 262176 | tf_op jit(solution)/shard_map/ppermute | solution.py:210
  66.1 3.1 %collective-permute-start.2 = (bf16[16,2048]{1,0:T(8,128)(2,1)S(1)}, bf16[16,2048]{1,0:T(8,128)(2,1)S(1)}, u32[]{:S(2)}, u32[]{:S(2)}) collective-permute-start(bf16[16,2048]{1,0:T(8,128)(2,1)S(1)} %get-tuple-element.19), channel_id=1, source_target_pairs={{0,2},{2,0},{4,6},{6,4},{1,3},{3,1},{5,7},{7,5},{8,10},{10,8},{12,... | collective-permute-start | bytes 196616 | tf_op jit(solution)/shard_map/ppermute | solution.py:210
  69.2 4.3 %collective-permute-start.3 = (bf16[16,2048]{1,0:T(8,128)(2,1)S(1)}, bf16[16,2048]{1,0:T(8,128)(2,1)S(1)}, u32[]{:S(2)}, u32[]{:S(2)}) collective-permute-start(bf16[16,2048]{1,0:T(8,128)(2,1)S(1)} %get-tuple-element.20), channel_id=1, source_target_pairs={{0,4},{2,6},{4,0},{6,2},{1,5},{3,7},{5,1},{7,3},{8,12},{10,14},{12... | collective-permute-start | bytes 196616 | tf_op jit(solution)/shard_map/ppermute | solution.py:210
  73.5 2.1 %collective-permute-start.4 = (bf16[16,2048]{1,0:T(8,128)(2,1)S(1)}, bf16[16,2048]{1,0:T(8,128)(2,1)S(1)}, u32[]{:S(2)}, u32[]{:S(2)}) collective-permute-start(bf16[16,2048]{1,0:T(8,128)(2,1)S(1)} %get-tuple-element.21), channel_id=1, source_target_pairs={{0,6},{2,4},{4,2},{6,0},{1,7},{3,5},{5,3},{7,1},{8,14},{10,12},{12... | collective-permute-start | bytes 196616 | tf_op jit(solution)/shard_map/ppermute | solution.py:210
  75.7 0.3 collective-permute-done.3.from_two
  76.0 3.7 %collective-permute-done.4.from_three = bf16[16,2048]{1,0:T(8,128)(2,1)S(1)} collective-permute-done((bf16[16,2048]{1,0:T(8,128)(2,1)S(1)}, bf16[16,2048]{1,0:T(8,128)(2,1)S(1)}, u32[]{:S(2)}, u32[]{:S(2)}) %collective-permute-start.4) | collective-permute-done | bytes 65568 | tf_op jit(solution)/shard_map/ppermute | solution.py:210
  79.8 0.8 %shard_map.96 = bf16[16,2048]{1,0:T(8,128)(2,1)} custom-call(f32[16,2048]{1,0:T(8,128)S(1)} %get-tuple-element.18.mine, bf16[16,2048]{1,0:T(8,128)(2,1)S(1)} %collective-permute-done.2.from_one, bf16[16,2048]{1,0:T(8,128)(2,1)S(1)} %collective-permute-done.3.from_two, bf16[16,2048]{1,0:T(8,128)(2,1)S(1)} %collective-permute-done.4.from_three, ...), custom_call_target="tpu_custom_call" | custom-call | flops 1000000 | bytes 4000000 | tf_op jit(solution)/shard_map/pallas_call | solution.py:190
  80.6 0.8 shard_map.98
  (12 shorter events, 0.1 us)
Async XLA Ops:
  0.6 21.8 %copy-start.2 = (bf16[256,256]{1,0:T(8,128)(2,1)S(1)}, bf16[256,256]{1,0:T(8,128)(2,1)}, u32[]{:S(2)}) copy-start(bf16[256,256]{1,0:T(8,128)(2,1)} %constant.2.clone.pick) | copy-start | bytes 393220
  0.6 21.8 %copy-start = (bf16[2048,352]{0,1:T(8,128)(2,1)S(1)}, bf16[2048,352]{0,1:T(8,128)(2,1)}, u32[]{:S(2)}) copy-start(bf16[2048,352]{0,1:T(8,128)(2,1)} %param.10) | copy-start | bytes 4325380
  0.7 21.8 %copy-start.3 = (f32[2048]{0:T(1024)S(1)}, f32[2048]{0:T(1024)}, u32[]{:S(2)}) copy-start(f32[2048]{0:T(1024)} %param.9) | copy-start | bytes 24580
  13.3 9.2 %collective-permute-start = (bf16[64,4096]{1,0:T(8,128)(2,1)S(1)}, bf16[64,4096]{1,0:T(8,128)(2,1)S(1)}, u32[]{:S(2)}, u32[]{:S(2)}) collective-permute-start(bf16[64,4096]{1,0:T(8,128)(2,1)S(1)} %bitcast.6), channel_id=1, source_target_pairs={{0,1},{1,0},{2,3},{3,2},{4,5},{5,4},{6,7},{7,6},{8,9},{9,8},{10,11... | collective-permute-start | bytes 1572872 | tf_op jit(solution)/shard_map/ppermute | solution.py:210
  26.8 19.6 %all-to-all-start.1 = ((bf16[32,8,256]{2,1,0:T(8,128)(2,1)}), bf16[32,8,256]{2,1,0:T(8,128)(2,1)S(1)}, u32[]{:S(2)}, u32[]{:S(2)}) async-start(bf16[32,8,256]{2,1,0:T(8,128)(2,1)} %get-tuple-element.26), calls=%async_computation.1 | async-start | bytes 262144 | tf_op jit(solution)/shard_map/all_to_all | solution.py:249
  30.7 8.7 %collective-permute-start.5 = (bf16[128,896]{1,0:T(8,128)(2,1)S(1)}, bf16[128,896]{1,0:T(8,128)(2,1)S(1)}, u32[]{:S(2)}, u32[]{:S(2)}) collective-permute-start(bf16[128,896]{1,0:T(8,128)(2,1)S(1)} %get-tuple-element.23), channel_id=1, source_target_pairs={{0,8},{8,0},{16,24},{24,16},{32,40},{40,32},{48,56},{56,48},{64,72... | collective-permute-start | bytes 688136 | tf_op jit(solution)/shard_map/ppermute | solution.py:210
  34.1 12.3 %collective-permute-start.6 = (bf16[128,896]{1,0:T(8,128)(2,1)S(1)}, bf16[128,896]{1,0:T(8,128)(2,1)S(1)}, u32[]{:S(2)}, u32[]{:S(2)}) collective-permute-start(bf16[128,896]{1,0:T(8,128)(2,1)S(1)} %get-tuple-element.24), channel_id=1, source_target_pairs={{0,64},{8,72},{16,80},{24,88},{32,96},{40,104},{48,112},{56,120},{... | collective-permute-start | bytes 688136 | tf_op jit(solution)/shard_map/ppermute | solution.py:210
  37.3 9.1 %collective-permute-start.7 = (bf16[128,896]{1,0:T(8,128)(2,1)S(1)}, bf16[128,896]{1,0:T(8,128)(2,1)S(1)}, u32[]{:S(2)}, u32[]{:S(2)}) collective-permute-start(bf16[128,896]{1,0:T(8,128)(2,1)S(1)} %get-tuple-element.25), channel_id=1, source_target_pairs={{0,72},{8,64},{16,88},{24,80},{32,104},{40,96},{48,120},{56,112},{... | collective-permute-start | bytes 688136 | tf_op jit(solution)/shard_map/ppermute | solution.py:210
  46.4 33.4 %copy-start.1 = (bf16[16,2048]{1,0:T(8,128)(2,1)S(1)}, bf16[16,2048]{1,0:T(8,128)(2,1)}, u32[]{:S(2)}) copy-start(bf16[16,2048]{1,0:T(8,128)(2,1)} %inputs.1) | copy-start | bytes 196612
  47.8 32.8 %all-to-all-start.2 = ((bf16[16,104,128]{2,1,0:T(8,128)(2,1)}), bf16[16,104,128]{2,1,0:T(8,128)(2,1)S(1)}, u32[]{:S(2)}, u32[]{:S(2)}) async-start(bf16[16,104,128]{2,1,0:T(8,128)(2,1)} %shard_map.97), calls=%async_computation.2 | async-start | bytes 851968 | tf_op jit(solution)/shard_map/all_to_all | solution.py:264
  60.2 5.9 %collective-permute-start.1 = (bf16[64,2048]{1,0:T(8,128)(2,1)S(1)}, bf16[64,2048]{1,0:T(8,128)(2,1)S(1)}, u32[]{:S(2)}, u32[]{:S(2)}) collective-permute-start(bf16[64,2048]{1,0:T(8,128)(2,1)S(1)} %get-tuple-element.17), channel_id=1, source_target_pairs={{0,1},{1,0},{2,3},{3,2},{4,5},{5,4},{6,7},{7,6},{8,9},{9,8},{10,11... | collective-permute-start | bytes 786440 | tf_op jit(solution)/shard_map/ppermute | solution.py:210
  66.1 9.6 %collective-permute-start.2 = (bf16[16,2048]{1,0:T(8,128)(2,1)S(1)}, bf16[16,2048]{1,0:T(8,128)(2,1)S(1)}, u32[]{:S(2)}, u32[]{:S(2)}) collective-permute-start(bf16[16,2048]{1,0:T(8,128)(2,1)S(1)} %get-tuple-element.19), channel_id=1, source_target_pairs={{0,2},{2,0},{4,6},{6,4},{1,3},{3,1},{5,7},{7,5},{8,10},{10,8},{12,... | collective-permute-start | bytes 196616 | tf_op jit(solution)/shard_map/ppermute | solution.py:210
  69.2 6.8 %collective-permute-start.3 = (bf16[16,2048]{1,0:T(8,128)(2,1)S(1)}, bf16[16,2048]{1,0:T(8,128)(2,1)S(1)}, u32[]{:S(2)}, u32[]{:S(2)}) collective-permute-start(bf16[16,2048]{1,0:T(8,128)(2,1)S(1)} %get-tuple-element.20), channel_id=1, source_target_pairs={{0,4},{2,6},{4,0},{6,2},{1,5},{3,7},{5,1},{7,3},{8,12},{10,14},{12... | collective-permute-start | bytes 196616 | tf_op jit(solution)/shard_map/ppermute | solution.py:210
  73.5 6.2 %collective-permute-start.4 = (bf16[16,2048]{1,0:T(8,128)(2,1)S(1)}, bf16[16,2048]{1,0:T(8,128)(2,1)S(1)}, u32[]{:S(2)}, u32[]{:S(2)}) collective-permute-start(bf16[16,2048]{1,0:T(8,128)(2,1)S(1)} %get-tuple-element.21), channel_id=1, source_target_pairs={{0,6},{2,4},{4,2},{6,0},{1,7},{3,5},{5,3},{7,1},{8,14},{10,12},{12... | collective-permute-start | bytes 196616 | tf_op jit(solution)/shard_map/ppermute | solution.py:210

commit v4 on v3

--- a/solution.py
+++ b/solution.py
@@ -10,6 +10,7 @@
 EPS = 1e-06
 SIDE = 8
 HALF = SIDE // 2
+FIRST_CHIP = 3
 EVERY = ("rep", "fs", "tp")
 OWN = ("fs", "tp")
 
@@ -23,9 +24,11 @@
     for zh in range(HALF)
     for yh in range(HALF)
 ]
-QUAD_DEVICES = [[8 * r + k for r in quad for k in range(8)] for quad in QUADS]
+QUAD_DEVICES = [
+    [8 * r + k for r in sorted(quad)[::-1] for k in (5, 3, 7, 1, 0, 2, 4, 6)] for quad in QUADS
+]
 FAR = [
-    [place(a, zh) * SIDE + place(b, yh) for zh in range(HALF) for yh in range(HALF)]
+    [place(a, zh) * SIDE + place(b, yh) for zh in range(HALF) for yh in range(HALF)][::-1]
     for a in range(2)
     for b in range(2)
 ]
@@ -140,11 +143,11 @@
             ),
             axis=0,
         )
-        blocks[k, :32] = mine[:, :128].astype(jnp.bfloat16)
-        blocks[k, 32:64] = mine[:, 128:256].astype(jnp.bfloat16)
-        blocks[k, 64:88] = rest.astype(jnp.bfloat16)
-        blocks[k, 88:96] = total[:, :128]
-        blocks[k, 96:] = total[:, 128:]
+        blocks[15 - k, :32] = mine[:, :128].astype(jnp.bfloat16)
+        blocks[15 - k, 32:64] = mine[:, 128:256].astype(jnp.bfloat16)
+        blocks[15 - k, 64:88] = rest.astype(jnp.bfloat16)
+        blocks[15 - k, 88:96] = total[:, :128]
+        blocks[15 - k, 96:] = total[:, 128:]
 
 
 def last_kernel(got, down, gain):
@@ -167,7 +170,7 @@
 def split_kernel(keep, got, mine, to_one, to_two, to_three):
     me = lax.axis_index("fs")
     for k, out in enumerate((mine, to_one, to_two, to_three)):
-        rows = pl.ds(pl.multiple_of(16 * (me ^ k), 16), 16)
+        rows = pl.ds(pl.multiple_of(16 * (me ^ k ^ FIRST_CHIP), 16), 16)
         out[...] = (keep[rows, :] + got[rows, :].astype(jnp.float32)).astype(out.dtype)
 
 
@@ -198,20 +201,21 @@
     )(*args)
 
 
-def to_all(array, axis):
-    count = lax.axis_size(axis)
-    return lax.all_to_all(
-        jnp.broadcast_to(array[None], (count, *array.shape)), axis, 0, 0, tiled=True
-    )
-
-
 def partner(array, axis, bit):
     count = lax.axis_size(axis)
     return lax.ppermute(array, axis, [(i, i ^ bit) for i in range(count)])
 
 
 def per_device(inputs, cotangent, norm_gain, gate_weight, up_weight, down_weight):
-    near = to_all(jnp.concatenate((inputs, cotangent), axis=1), "fs").reshape(64, 4096)
+    own = jnp.concatenate((inputs, cotangent), axis=1)
+    near = lax.all_to_all(
+        jnp.broadcast_to(own[None], (4, *own.shape)),
+        "fs",
+        0,
+        0,
+        tiled=True,
+        axis_index_groups=[[k ^ FIRST_CHIP for k in range(4)]],
+    ).reshape(64, 4096)
     other = partner(near, "tp", 1)
     pick = jnp.asarray(one_row_of_quads(), jnp.bfloat16)
     block = ((128, 896), jnp.bfloat16)

time: 82.8 us -> 82 us (level)
  the two profiles are of different devices: /device:TPU:1 before, /device:TPU:72 now
where the time goes in v4:
time: 82 us; the launch traced here: 81.4 us
  starting transfers between devices  44.8 us (55%)
  waiting for transfers between devices  14.4 us (18%)
  blocking collectives  12.8 us (16%)
  Pallas kernels  7.45 us (9%)
  other arithmetic  1 us (1%)
    ppermute x8, starting transfers between devices, partner(): return lax.ppermute(array, axis, [(i, i ^ bit) for i in range(count)])  23.5 us
    all_to_all x1, starting transfers between devices, per_device(): got = lax.all_to_all(blocks, 'rep', 0, 0, tiled=True, axis_index_groups=FAR)  14.9 us
    ppermute x8, waiting for transfers between devices, partner(): return lax.ppermute(array, axis, [(i, i ^ bit) for i in range(count)])  14.4 us
    all_to_all x1, blocking collectives, per_device(): lax.all_to_all(jnp.broadcast_to(own[None], (4, *own.shape)), 'fs', 0, 0,...  12.8 us
    pallas_call x5, Pallas kernels, call(): pl.pallas_call(body, out_shape=out, in_specs=[whole] * (len(args) - left)...  7.45 us
    all_to_all x1, starting transfers between devices, per_device(): lax.all_to_all(part_gain, EVERY, 0, 0, tiled=True, axis_index_groups=QUAD...  6.5 us
  transfers between devices with their start and end apart: 10, of which 5 were waited for; matrix products, arithmetic and copies ran while one was open for 0% of the time, Pallas kernels for 1%

profile of v4, /device:TPU:72, one launch (start us, length us, event | category | flops | bytes accessed | tf_op | source)
XLA Modules:
  0.0 81.4 jit_solution(17833466873567447077)
XLA Ops:
  0.6 0.0 copy-start.2
  0.7 1.0 %pad_maximum_fusion = bf16[16,4096]{1,0:T(8,128)(2,1)S(1)} fusion(bf16[16,2048]{1,0:T(8,128)(2,1)} %param.8, bf16[16,2048]{1,0:T(8,128)(2,1)} %inputs.1), kind=kLoop, calls=%fused_computation | loop fusion | flops 262144 | bytes 262144 | tf_op jit(solution)/shard_map/concatenate | solution.py:210
  1.7 12.8 %all_to_all.15 = bf16[4,16,4096]{2,1,0:T(8,128)(2,1)S(1)} all-to-all(bf16[4,16,4096]{2,1,0:T(8,128)(2,1)S(1)} %broadcast_in_dim.2), channel_id=1, replica_groups={{6,4,2,0},{7,5,3,1},{14,12,10,8},{15,13,11,9},{22,20,18,16},{23,21,19,1..., dimensions={0} | all-to-all | bytes 1048576 | tf_op jit(solution)/shard_map/all_to_all | solution.py:211
  14.6 1.9 %collective-permute-start = (bf16[64,4096]{1,0:T(8,128)(2,1)S(1)}, bf16[64,4096]{1,0:T(8,128)(2,1)S(1)}, u32[]{:S(2)}, u32[]{:S(2)}) collective-permute-start(bf16[64,4096]{1,0:T(8,128)(2,1)S(1)} %bitcast.6), channel_id=1, source_target_pairs={{0,1},{1,0},{2,3},{3,2},{4,5},{5,4},{6,7},{7,6},{8,9},{9,8},{10,11... | collective-permute-start | bytes 1572872 | tf_op jit(solution)/shard_map/ppermute | solution.py:206
  16.5 1.9 %collective-permute-done.far = bf16[64,4096]{1,0:T(8,128)(2,1)S(1)} collective-permute-done((bf16[64,4096]{1,0:T(8,128)(2,1)S(1)}, bf16[64,4096]{1,0:T(8,128)(2,1)S(1)}, u32[]{:S(2)}, u32[]{:S(2)}) %collective-permute-start) | collective-permute-done | bytes 524320 | tf_op jit(solution)/shard_map/ppermute | solution.py:206
  18.4 4.4 %shard_map.94 = (bf16[128,896]{1,0:T(8,128)(2,1)S(1)}, bf16[128,896]{1,0:T(8,128)(2,1)S(1)}, bf16[128,896]{1,0:T(8,128)(2,1)S(1)}, bf16[128,896]{1,0:T(8,128)(2,...) custom-call(bf16[64,4096]{1,0:T(8,128)(2,1)S(1)} %bitcast.7, ...), custom_call_target="tpu_custom_call" | custom-call | flops 1000000000 | bytes 4000000 | tf_op jit(solution)/shard_map/pallas_call | solution.py:193
  22.7 6.5 %all-to-all-start.1 = ((bf16[32,8,256]{2,1,0:T(8,128)(2,1)}), bf16[32,8,256]{2,1,0:T(8,128)(2,1)S(1)}, u32[]{:S(2)}, u32[]{:S(2)}) async-start(bf16[32,8,256]{2,1,0:T(8,128)(2,1)} %get-tuple-element.26), calls=%async_computation.1 | async-start | bytes 262144 | tf_op jit(solution)/shard_map/all_to_all | solution.py:253
  29.2 3.4 %collective-permute-start.5 = (bf16[128,896]{1,0:T(8,128)(2,1)S(1)}, bf16[128,896]{1,0:T(8,128)(2,1)S(1)}, u32[]{:S(2)}, u32[]{:S(2)}) collective-permute-start(bf16[128,896]{1,0:T(8,128)(2,1)S(1)} %get-tuple-element.23), channel_id=1, source_target_pairs={{0,8},{8,0},{16,24},{24,16},{32,40},{40,32},{48,56},{56,48},{64,72... | collective-permute-start | bytes 688136 | tf_op jit(solution)/shard_map/ppermute | solution.py:206
  32.6 3.4 %collective-permute-start.6 = (bf16[128,896]{1,0:T(8,128)(2,1)S(1)}, bf16[128,896]{1,0:T(8,128)(2,1)S(1)}, u32[]{:S(2)}, u32[]{:S(2)}) collective-permute-start(bf16[128,896]{1,0:T(8,128)(2,1)S(1)} %get-tuple-element.24), channel_id=1, source_target_pairs={{0,64},{8,72},{16,80},{24,88},{32,96},{40,104},{48,112},{56,120},{... | collective-permute-start | bytes 688136 | tf_op jit(solution)/shard_map/ppermute | solution.py:206
  36.1 2.4 %collective-permute-start.7 = (bf16[128,896]{1,0:T(8,128)(2,1)S(1)}, bf16[128,896]{1,0:T(8,128)(2,1)S(1)}, u32[]{:S(2)}, u32[]{:S(2)}) collective-permute-start(bf16[128,896]{1,0:T(8,128)(2,1)S(1)} %get-tuple-element.25), channel_id=1, source_target_pairs={{0,72},{8,64},{16,88},{24,80},{32,104},{40,96},{48,120},{56,112},{... | collective-permute-start | bytes 688136 | tf_op jit(solution)/shard_map/ppermute | solution.py:206
  38.5 0.3 collective-permute-done.5.got_y
  38.8 8.0 %collective-permute-done.6.got_z = bf16[128,896]{1,0:T(8,128)(2,1)S(1)} collective-permute-done((bf16[128,896]{1,0:T(8,128)(2,1)S(1)}, bf16[128,896]{1,0:T(8,128)(2,1)S(1)}, u32[]{:S(2)}, u32[]{:S(2)}) %collective-permute-start.6) | collective-permute-done | bytes 229408 | tf_op jit(solution)/shard_map/ppermute | solution.py:206
  46.8 1.4 %shard_map.97 = bf16[16,104,128]{2,1,0:T(8,128)(2,1)} custom-call(bf16[128,896]{1,0:T(8,128)(2,1)S(1)} %get-tuple-element.22.own, bf16[128,896]{1,0:T(8,128)(2,1)S(1)} %collective-permute-done.5.got_y, bf16[128,896]{1,0:T(8,128)(2,1)S(1)} %collective-permute-done.6.got_z, bf16[128,896]{1,0:T(8,128)(2,1)S(1)} %collective-permute-done.7.got_zy, ...), custom_call_target="tpu_custom_call" | custom-call | flops 1000000 | bytes 4000000 | tf_op jit(solution)/shard_map/pallas_call | solution.py:193
  48.2 14.9 %all-to-all-start.2 = ((bf16[16,104,128]{2,1,0:T(8,128)(2,1)}), bf16[16,104,128]{2,1,0:T(8,128)(2,1)S(1)}, u32[]{:S(2)}, u32[]{:S(2)}) async-start(bf16[16,104,128]{2,1,0:T(8,128)(2,1)} %shard_map.97), calls=%async_computation.2 | async-start | bytes 851968 | tf_op jit(solution)/shard_map/all_to_all | solution.py:268
  63.1 1.9 %collective-permute-start.1 = (bf16[64,2048]{1,0:T(8,128)(2,1)S(1)}, bf16[64,2048]{1,0:T(8,128)(2,1)S(1)}, u32[]{:S(2)}, u32[]{:S(2)}) collective-permute-start(bf16[64,2048]{1,0:T(8,128)(2,1)S(1)} %get-tuple-element.17), channel_id=1, source_target_pairs={{0,1},{1,0},{2,3},{3,2},{4,5},{5,4},{6,7},{7,6},{8,9},{9,8},{10,11... | collective-permute-start | bytes 786440 | tf_op jit(solution)/shard_map/ppermute | solution.py:206
  65.0 1.5 %collective-permute-done.1.got = bf16[64,2048]{1,0:T(8,128)(2,1)S(1)} collective-permute-done((bf16[64,2048]{1,0:T(8,128)(2,1)S(1)}, bf16[64,2048]{1,0:T(8,128)(2,1)S(1)}, u32[]{:S(2)}, u32[]{:S(2)}) %collective-permute-start.1) | collective-permute-done | bytes 262176 | tf_op jit(solution)/shard_map/ppermute | solution.py:206
  66.6 1.9 %collective-permute-start.2 = (bf16[16,2048]{1,0:T(8,128)(2,1)S(1)}, bf16[16,2048]{1,0:T(8,128)(2,1)S(1)}, u32[]{:S(2)}, u32[]{:S(2)}) collective-permute-start(bf16[16,2048]{1,0:T(8,128)(2,1)S(1)} %get-tuple-element.19), channel_id=1, source_target_pairs={{0,2},{2,0},{4,6},{6,4},{1,3},{3,1},{5,7},{7,5},{8,10},{10,8},{12,... | collective-permute-start | bytes 196616 | tf_op jit(solution)/shard_map/ppermute | solution.py:206
  68.5 3.9 %collective-permute-start.3 = (bf16[16,2048]{1,0:T(8,128)(2,1)S(1)}, bf16[16,2048]{1,0:T(8,128)(2,1)S(1)}, u32[]{:S(2)}, u32[]{:S(2)}) collective-permute-start(bf16[16,2048]{1,0:T(8,128)(2,1)S(1)} %get-tuple-element.20), channel_id=1, source_target_pairs={{0,4},{2,6},{4,0},{6,2},{1,5},{3,7},{5,1},{7,3},{8,12},{10,14},{12... | collective-permute-start | bytes 196616 | tf_op jit(solution)/shard_map/ppermute | solution.py:206
  72.4 4.6 %collective-permute-start.4 = (bf16[16,2048]{1,0:T(8,128)(2,1)S(1)}, bf16[16,2048]{1,0:T(8,128)(2,1)S(1)}, u32[]{:S(2)}, u32[]{:S(2)}) collective-permute-start(bf16[16,2048]{1,0:T(8,128)(2,1)S(1)} %get-tuple-element.21), channel_id=1, source_target_pairs={{0,6},{2,4},{4,2},{6,0},{1,7},{3,5},{5,3},{7,1},{8,14},{10,12},{12... | collective-permute-start | bytes 196616 | tf_op jit(solution)/shard_map/ppermute | solution.py:206
  77.0 0.0 collective-permute-done.3.from_two
  77.0 2.8 %collective-permute-done.4.from_three = bf16[16,2048]{1,0:T(8,128)(2,1)S(1)} collective-permute-done((bf16[16,2048]{1,0:T(8,128)(2,1)S(1)}, bf16[16,2048]{1,0:T(8,128)(2,1)S(1)}, u32[]{:S(2)}, u32[]{:S(2)}) %collective-permute-start.4) | collective-permute-done | bytes 65568 | tf_op jit(solution)/shard_map/ppermute | solution.py:206
  79.8 0.8 %shard_map.96 = bf16[16,2048]{1,0:T(8,128)(2,1)} custom-call(f32[16,2048]{1,0:T(8,128)S(1)} %get-tuple-element.18.mine, bf16[16,2048]{1,0:T(8,128)(2,1)S(1)} %collective-permute-done.2.from_one, bf16[16,2048]{1,0:T(8,128)(2,1)S(1)} %collective-permute-done.3.from_two, bf16[16,2048]{1,0:T(8,128)(2,1)S(1)} %collective-permute-done.4.from_three, ...), custom_call_target="tpu_custom_call" | custom-call | flops 1000000 | bytes 4000000 | tf_op jit(solution)/shard_map/pallas_call | solution.py:193
  80.6 0.0 all-to-all-done.2.got
  80.6 0.8 shard_map.98
  (12 shorter events, 0.1 us)
Async XLA Ops:
  0.6 17.7 %copy-start.2 = (bf16[256,256]{1,0:T(8,128)(2,1)S(1)}, bf16[256,256]{1,0:T(8,128)(2,1)}, u32[]{:S(2)}) copy-start(bf16[256,256]{1,0:T(8,128)(2,1)} %constant.2.clone.pick) | copy-start | bytes 393220
  0.6 17.7 %copy-start = (bf16[2048,352]{0,1:T(8,128)(2,1)S(1)}, bf16[2048,352]{0,1:T(8,128)(2,1)}, u32[]{:S(2)}) copy-start(bf16[2048,352]{0,1:T(8,128)(2,1)} %param.10) | copy-start | bytes 4325380
  0.7 17.7 %copy-start.3 = (f32[2048]{0:T(1024)S(1)}, f32[2048]{0:T(1024)}, u32[]{:S(2)}) copy-start(f32[2048]{0:T(1024)} %param.9) | copy-start | bytes 24580
  14.6 3.8 %collective-permute-start = (bf16[64,4096]{1,0:T(8,128)(2,1)S(1)}, bf16[64,4096]{1,0:T(8,128)(2,1)S(1)}, u32[]{:S(2)}, u32[]{:S(2)}) collective-permute-start(bf16[64,4096]{1,0:T(8,128)(2,1)S(1)} %bitcast.6), channel_id=1, source_target_pairs={{0,1},{1,0},{2,3},{3,2},{4,5},{5,4},{6,7},{7,6},{8,9},{9,8},{10,11... | collective-permute-start | bytes 1572872 | tf_op jit(solution)/shard_map/ppermute | solution.py:206
  22.7 24.0 %all-to-all-start.1 = ((bf16[32,8,256]{2,1,0:T(8,128)(2,1)}), bf16[32,8,256]{2,1,0:T(8,128)(2,1)S(1)}, u32[]{:S(2)}, u32[]{:S(2)}) async-start(bf16[32,8,256]{2,1,0:T(8,128)(2,1)} %get-tuple-element.26), calls=%async_computation.1 | async-start | bytes 262144 | tf_op jit(solution)/shard_map/all_to_all | solution.py:253
  29.2 9.5 %collective-permute-start.5 = (bf16[128,896]{1,0:T(8,128)(2,1)S(1)}, bf16[128,896]{1,0:T(8,128)(2,1)S(1)}, u32[]{:S(2)}, u32[]{:S(2)}) collective-permute-start(bf16[128,896]{1,0:T(8,128)(2,1)S(1)} %get-tuple-element.23), channel_id=1, source_target_pairs={{0,8},{8,0},{16,24},{24,16},{32,40},{40,32},{48,56},{56,48},{64,72... | collective-permute-start | bytes 688136 | tf_op jit(solution)/shard_map/ppermute | solution.py:206
  32.6 14.2 %collective-permute-start.6 = (bf16[128,896]{1,0:T(8,128)(2,1)S(1)}, bf16[128,896]{1,0:T(8,128)(2,1)S(1)}, u32[]{:S(2)}, u32[]{:S(2)}) collective-permute-start(bf16[128,896]{1,0:T(8,128)(2,1)S(1)} %get-tuple-element.24), channel_id=1, source_target_pairs={{0,64},{8,72},{16,80},{24,88},{32,96},{40,104},{48,112},{56,120},{... | collective-permute-start | bytes 688136 | tf_op jit(solution)/shard_map/ppermute | solution.py:206
  36.1 10.7 %collective-permute-start.7 = (bf16[128,896]{1,0:T(8,128)(2,1)S(1)}, bf16[128,896]{1,0:T(8,128)(2,1)S(1)}, u32[]{:S(2)}, u32[]{:S(2)}) collective-permute-start(bf16[128,896]{1,0:T(8,128)(2,1)S(1)} %get-tuple-element.25), channel_id=1, source_target_pairs={{0,72},{8,64},{16,88},{24,80},{32,104},{40,96},{48,120},{56,112},{... | collective-permute-start | bytes 688136 | tf_op jit(solution)/shard_map/ppermute | solution.py:206
  46.8 33.0 %copy-start.1 = (bf16[16,2048]{1,0:T(8,128)(2,1)S(1)}, bf16[16,2048]{1,0:T(8,128)(2,1)}, u32[]{:S(2)}) copy-start(bf16[16,2048]{1,0:T(8,128)(2,1)} %inputs.1) | copy-start | bytes 196612
  48.2 32.4 %all-to-all-start.2 = ((bf16[16,104,128]{2,1,0:T(8,128)(2,1)}), bf16[16,104,128]{2,1,0:T(8,128)(2,1)S(1)}, u32[]{:S(2)}, u32[]{:S(2)}) async-start(bf16[16,104,128]{2,1,0:T(8,128)(2,1)} %shard_map.97), calls=%async_computation.2 | async-start | bytes 851968 | tf_op jit(solution)/shard_map/all_to_all | solution.py:268
  63.1 3.4 %collective-permute-start.1 = (bf16[64,2048]{1,0:T(8,128)(2,1)S(1)}, bf16[64,2048]{1,0:T(8,128)(2,1)S(1)}, u32[]{:S(2)}, u32[]{:S(2)}) collective-permute-start(bf16[64,2048]{1,0:T(8,128)(2,1)S(1)} %get-tuple-element.17), channel_id=1, source_target_pairs={{0,1},{1,0},{2,3},{3,2},{4,5},{5,4},{6,7},{7,6},{8,9},{9,8},{10,11... | collective-permute-start | bytes 786440 | tf_op jit(solution)/shard_map/ppermute | solution.py:206
  66.6 10.4 %collective-permute-start.2 = (bf16[16,2048]{1,0:T(8,128)(2,1)S(1)}, bf16[16,2048]{1,0:T(8,128)(2,1)S(1)}, u32[]{:S(2)}, u32[]{:S(2)}) collective-permute-start(bf16[16,2048]{1,0:T(8,128)(2,1)S(1)} %get-tuple-element.19), channel_id=1, source_target_pairs={{0,2},{2,0},{4,6},{6,4},{1,3},{3,1},{5,7},{7,5},{8,10},{10,8},{12,... | collective-permute-start | bytes 196616 | tf_op jit(solution)/shard_map/ppermute | solution.py:206
  68.5 8.5 %collective-permute-start.3 = (bf16[16,2048]{1,0:T(8,128)(2,1)S(1)}, bf16[16,2048]{1,0:T(8,128)(2,1)S(1)}, u32[]{:S(2)}, u32[]{:S(2)}) collective-permute-start(bf16[16,2048]{1,0:T(8,128)(2,1)S(1)} %get-tuple-element.20), channel_id=1, source_target_pairs={{0,4},{2,6},{4,0},{6,2},{1,5},{3,7},{5,1},{7,3},{8,12},{10,14},{12... | collective-permute-start | bytes 196616 | tf_op jit(solution)/shard_map/ppermute | solution.py:206
  72.4 7.4 %collective-permute-start.4 = (bf16[16,2048]{1,0:T(8,128)(2,1)S(1)}, bf16[16,2048]{1,0:T(8,128)(2,1)S(1)}, u32[]{:S(2)}, u32[]{:S(2)}) collective-permute-start(bf16[16,2048]{1,0:T(8,128)(2,1)S(1)} %get-tuple-element.21), channel_id=1, source_target_pairs={{0,6},{2,4},{4,2},{6,0},{1,7},{3,5},{5,3},{7,1},{8,14},{10,12},{12... | collective-permute-start | bytes 196616 | tf_op jit(solution)/shard_map/ppermute | solution.py:206

commit v5 on v4

--- a/solution.py
+++ b/solution.py
@@ -27,11 +27,13 @@
 QUAD_DEVICES = [
     [8 * r + k for r in sorted(quad)[::-1] for k in (5, 3, 7, 1, 0, 2, 4, 6)] for quad in QUADS
 ]
+FAR_ORDER = tuple(HALF * zh + yh for yh in (3, 2, 1, 0) for zh in (3, 2, 1, 0))
 FAR = [
-    [place(a, zh) * SIDE + place(b, yh) for zh in range(HALF) for yh in range(HALF)][::-1]
+    [place(a, k // HALF) * SIDE + place(b, k % HALF) for k in FAR_ORDER]
     for a in range(2)
     for b in range(2)
 ]
+PLACES = [FAR_ORDER.index(k) for k in range(HALF * HALF)]
 
 
 def one_row_of_quads():
@@ -143,11 +145,11 @@
             ),
             axis=0,
         )
-        blocks[15 - k, :32] = mine[:, :128].astype(jnp.bfloat16)
-        blocks[15 - k, 32:64] = mine[:, 128:256].astype(jnp.bfloat16)
-        blocks[15 - k, 64:88] = rest.astype(jnp.bfloat16)
-        blocks[15 - k, 88:96] = total[:, :128]
-        blocks[15 - k, 96:] = total[:, 128:]
+        blocks[PLACES[k], :32] = mine[:, :128].astype(jnp.bfloat16)
+        blocks[PLACES[k], 32:64] = mine[:, 128:256].astype(jnp.bfloat16)
+        blocks[PLACES[k], 64:88] = rest.astype(jnp.bfloat16)
+        blocks[PLACES[k], 88:96] = total[:, :128]
+        blocks[PLACES[k], 96:] = total[:, 128:]
 
 
 def last_kernel(got, down, gain):

time: 82 us -> 82 us (level)
  no operation moved by 1% of the time
where the time goes in v5:
time: 82 us; the launch traced here: 81.4 us
  starting transfers between devices  44.8 us (55%)
  waiting for transfers between devices  14.4 us (18%)
  blocking collectives  12.8 us (16%)
  Pallas kernels  7.45 us (9%)
  other arithmetic  1 us (1%)
    ppermute x8, starting transfers between devices, partner(): return lax.ppermute(array, axis, [(i, i ^ bit) for i in range(count)])  23.5 us
    all_to_all x1, starting transfers between devices, per_device(): got = lax.all_to_all(blocks, 'rep', 0, 0, tiled=True, axis_index_groups=FAR)  14.9 us
    ppermute x8, waiting for transfers between devices, partner(): return lax.ppermute(array, axis, [(i, i ^ bit) for i in range(count)])  14.4 us
    all_to_all x1, blocking collectives, per_device(): lax.all_to_all(jnp.broadcast_to(own[None], (4, *own.shape)), 'fs', 0, 0,...  12.8 us
    pallas_call x5, Pallas kernels, call(): pl.pallas_call(body, out_shape=out, in_specs=[whole] * (len(args) - left)...  7.45 us
    all_to_all x1, starting transfers between devices, per_device(): lax.all_to_all(part_gain, EVERY, 0, 0, tiled=True, axis_index_groups=QUAD...  6.5 us
  transfers between devices with their start and end apart: 10, of which 5 were waited for; matrix products, arithmetic and copies ran while one was open for 0% of the time, Pallas kernels for 1%

profile of v5, /device:TPU:72, one launch (start us, length us, event | category | flops | bytes accessed | tf_op | source)
XLA Modules:
  0.0 81.4 jit_solution(3438414384688812456)
XLA Ops:
  0.6 0.0 copy-start.2
  0.7 1.0 %pad_maximum_fusion = bf16[16,4096]{1,0:T(8,128)(2,1)S(1)} fusion(bf16[16,2048]{1,0:T(8,128)(2,1)} %param.8, bf16[16,2048]{1,0:T(8,128)(2,1)} %inputs.1), kind=kLoop, calls=%fused_computation | loop fusion | flops 262144 | bytes 262144 | tf_op jit(solution)/shard_map/concatenate | solution.py:212
  1.7 12.8 %all_to_all.15 = bf16[4,16,4096]{2,1,0:T(8,128)(2,1)S(1)} all-to-all(bf16[4,16,4096]{2,1,0:T(8,128)(2,1)S(1)} %broadcast_in_dim.2), channel_id=1, replica_groups={{6,4,2,0},{7,5,3,1},{14,12,10,8},{15,13,11,9},{22,20,18,16},{23,21,19,1..., dimensions={0} | all-to-all | bytes 1048576 | tf_op jit(solution)/shard_map/all_to_all | solution.py:213
  14.6 1.9 %collective-permute-start = (bf16[64,4096]{1,0:T(8,128)(2,1)S(1)}, bf16[64,4096]{1,0:T(8,128)(2,1)S(1)}, u32[]{:S(2)}, u32[]{:S(2)}) collective-permute-start(bf16[64,4096]{1,0:T(8,128)(2,1)S(1)} %bitcast.6), channel_id=1, source_target_pairs={{0,1},{1,0},{2,3},{3,2},{4,5},{5,4},{6,7},{7,6},{8,9},{9,8},{10,11... | collective-permute-start | bytes 1572872 | tf_op jit(solution)/shard_map/ppermute | solution.py:208
  16.5 1.9 %collective-permute-done.far = bf16[64,4096]{1,0:T(8,128)(2,1)S(1)} collective-permute-done((bf16[64,4096]{1,0:T(8,128)(2,1)S(1)}, bf16[64,4096]{1,0:T(8,128)(2,1)S(1)}, u32[]{:S(2)}, u32[]{:S(2)}) %collective-permute-start) | collective-permute-done | bytes 524320 | tf_op jit(solution)/shard_map/ppermute | solution.py:208
  18.4 4.4 %shard_map.94 = (bf16[128,896]{1,0:T(8,128)(2,1)S(1)}, bf16[128,896]{1,0:T(8,128)(2,1)S(1)}, bf16[128,896]{1,0:T(8,128)(2,1)S(1)}, bf16[128,896]{1,0:T(8,128)(2,...) custom-call(bf16[64,4096]{1,0:T(8,128)(2,1)S(1)} %bitcast.7, ...), custom_call_target="tpu_custom_call" | custom-call | flops 1000000000 | bytes 4000000 | tf_op jit(solution)/shard_map/pallas_call | solution.py:195
  22.7 6.5 %all-to-all-start.1 = ((bf16[32,8,256]{2,1,0:T(8,128)(2,1)}), bf16[32,8,256]{2,1,0:T(8,128)(2,1)S(1)}, u32[]{:S(2)}, u32[]{:S(2)}) async-start(bf16[32,8,256]{2,1,0:T(8,128)(2,1)} %get-tuple-element.26), calls=%async_computation.1 | async-start | bytes 262144 | tf_op jit(solution)/shard_map/all_to_all | solution.py:255
  29.2 3.4 %collective-permute-start.5 = (bf16[128,896]{1,0:T(8,128)(2,1)S(1)}, bf16[128,896]{1,0:T(8,128)(2,1)S(1)}, u32[]{:S(2)}, u32[]{:S(2)}) collective-permute-start(bf16[128,896]{1,0:T(8,128)(2,1)S(1)} %get-tuple-element.23), channel_id=1, source_target_pairs={{0,8},{8,0},{16,24},{24,16},{32,40},{40,32},{48,56},{56,48},{64,72... | collective-permute-start | bytes 688136 | tf_op jit(solution)/shard_map/ppermute | solution.py:208
  32.6 3.4 %collective-permute-start.6 = (bf16[128,896]{1,0:T(8,128)(2,1)S(1)}, bf16[128,896]{1,0:T(8,128)(2,1)S(1)}, u32[]{:S(2)}, u32[]{:S(2)}) collective-permute-start(bf16[128,896]{1,0:T(8,128)(2,1)S(1)} %get-tuple-element.24), channel_id=1, source_target_pairs={{0,64},{8,72},{16,80},{24,88},{32,96},{40,104},{48,112},{56,120},{... | collective-permute-start | bytes 688136 | tf_op jit(solution)/shard_map/ppermute | solution.py:208
  36.1 2.4 %collective-permute-start.7 = (bf16[128,896]{1,0:T(8,128)(2,1)S(1)}, bf16[128,896]{1,0:T(8,128)(2,1)S(1)}, u32[]{:S(2)}, u32[]{:S(2)}) collective-permute-start(bf16[128,896]{1,0:T(8,128)(2,1)S(1)} %get-tuple-element.25), channel_id=1, source_target_pairs={{0,72},{8,64},{16,88},{24,80},{32,104},{40,96},{48,120},{56,112},{... | collective-permute-start | bytes 688136 | tf_op jit(solution)/shard_map/ppermute | solution.py:208
  38.5 0.3 collective-permute-done.5.got_y
  38.8 8.0 %collective-permute-done.6.got_z = bf16[128,896]{1,0:T(8,128)(2,1)S(1)} collective-permute-done((bf16[128,896]{1,0:T(8,128)(2,1)S(1)}, bf16[128,896]{1,0:T(8,128)(2,1)S(1)}, u32[]{:S(2)}, u32[]{:S(2)}) %collective-permute-start.6) | collective-permute-done | bytes 229408 | tf_op jit(solution)/shard_map/ppermute | solution.py:208
  46.8 1.4 %shard_map.97 = bf16[16,104,128]{2,1,0:T(8,128)(2,1)} custom-call(bf16[128,896]{1,0:T(8,128)(2,1)S(1)} %get-tuple-element.22.own, bf16[128,896]{1,0:T(8,128)(2,1)S(1)} %collective-permute-done.5.got_y, bf16[128,896]{1,0:T(8,128)(2,1)S(1)} %collective-permute-done.6.got_z, bf16[128,896]{1,0:T(8,128)(2,1)S(1)} %collective-permute-done.7.got_zy, ...), custom_call_target="tpu_custom_call" | custom-call | flops 1000000 | bytes 4000000 | tf_op jit(solution)/shard_map/pallas_call | solution.py:195
  48.2 14.9 %all-to-all-start.2 = ((bf16[16,104,128]{2,1,0:T(8,128)(2,1)}), bf16[16,104,128]{2,1,0:T(8,128)(2,1)S(1)}, u32[]{:S(2)}, u32[]{:S(2)}) async-start(bf16[16,104,128]{2,1,0:T(8,128)(2,1)} %shard_map.97), calls=%async_computation.2 | async-start | bytes 851968 | tf_op jit(solution)/shard_map/all_to_all | solution.py:270
  63.1 1.9 %collective-permute-start.1 = (bf16[64,2048]{1,0:T(8,128)(2,1)S(1)}, bf16[64,2048]{1,0:T(8,128)(2,1)S(1)}, u32[]{:S(2)}, u32[]{:S(2)}) collective-permute-start(bf16[64,2048]{1,0:T(8,128)(2,1)S(1)} %get-tuple-element.17), channel_id=1, source_target_pairs={{0,1},{1,0},{2,3},{3,2},{4,5},{5,4},{6,7},{7,6},{8,9},{9,8},{10,11... | collective-permute-start | bytes 786440 | tf_op jit(solution)/shard_map/ppermute | solution.py:208
  65.0 1.5 %collective-permute-done.1.got = bf16[64,2048]{1,0:T(8,128)(2,1)S(1)} collective-permute-done((bf16[64,2048]{1,0:T(8,128)(2,1)S(1)}, bf16[64,2048]{1,0:T(8,128)(2,1)S(1)}, u32[]{:S(2)}, u32[]{:S(2)}) %collective-permute-start.1) | collective-permute-done | bytes 262176 | tf_op jit(solution)/shard_map/ppermute | solution.py:208
  66.6 1.9 %collective-permute-start.2 = (bf16[16,2048]{1,0:T(8,128)(2,1)S(1)}, bf16[16,2048]{1,0:T(8,128)(2,1)S(1)}, u32[]{:S(2)}, u32[]{:S(2)}) collective-permute-start(bf16[16,2048]{1,0:T(8,128)(2,1)S(1)} %get-tuple-element.19), channel_id=1, source_target_pairs={{0,2},{2,0},{4,6},{6,4},{1,3},{3,1},{5,7},{7,5},{8,10},{10,8},{12,... | collective-permute-start | bytes 196616 | tf_op jit(solution)/shard_map/ppermute | solution.py:208
  68.5 3.9 %collective-permute-start.3 = (bf16[16,2048]{1,0:T(8,128)(2,1)S(1)}, bf16[16,2048]{1,0:T(8,128)(2,1)S(1)}, u32[]{:S(2)}, u32[]{:S(2)}) collective-permute-start(bf16[16,2048]{1,0:T(8,128)(2,1)S(1)} %get-tuple-element.20), channel_id=1, source_target_pairs={{0,4},{2,6},{4,0},{6,2},{1,5},{3,7},{5,1},{7,3},{8,12},{10,14},{12... | collective-permute-start | bytes 196616 | tf_op jit(solution)/shard_map/ppermute | solution.py:208
  72.4 4.6 %collective-permute-start.4 = (bf16[16,2048]{1,0:T(8,128)(2,1)S(1)}, bf16[16,2048]{1,0:T(8,128)(2,1)S(1)}, u32[]{:S(2)}, u32[]{:S(2)}) collective-permute-start(bf16[16,2048]{1,0:T(8,128)(2,1)S(1)} %get-tuple-element.21), channel_id=1, source_target_pairs={{0,6},{2,4},{4,2},{6,0},{1,7},{3,5},{5,3},{7,1},{8,14},{10,12},{12... | collective-permute-start | bytes 196616 | tf_op jit(solution)/shard_map/ppermute | solution.py:208
  77.0 0.0 collective-permute-done.3.from_two
  77.0 2.8 %collective-permute-done.4.from_three = bf16[16,2048]{1,0:T(8,128)(2,1)S(1)} collective-permute-done((bf16[16,2048]{1,0:T(8,128)(2,1)S(1)}, bf16[16,2048]{1,0:T(8,128)(2,1)S(1)}, u32[]{:S(2)}, u32[]{:S(2)}) %collective-permute-start.4) | collective-permute-done | bytes 65568 | tf_op jit(solution)/shard_map/ppermute | solution.py:208
  79.8 0.8 %shard_map.96 = bf16[16,2048]{1,0:T(8,128)(2,1)} custom-call(f32[16,2048]{1,0:T(8,128)S(1)} %get-tuple-element.18.mine, bf16[16,2048]{1,0:T(8,128)(2,1)S(1)} %collective-permute-done.2.from_one, bf16[16,2048]{1,0:T(8,128)(2,1)S(1)} %collective-permute-done.3.from_two, bf16[16,2048]{1,0:T(8,128)(2,1)S(1)} %collective-permute-done.4.from_three, ...), custom_call_target="tpu_custom_call" | custom-call | flops 1000000 | bytes 4000000 | tf_op jit(solution)/shard_map/pallas_call | solution.py:195
  80.6 0.0 all-to-all-done.2.got
  80.6 0.8 shard_map.98
  (12 shorter events, 0.1 us)
Async XLA Ops:
  0.6 17.7 %copy-start.2 = (bf16[256,256]{1,0:T(8,128)(2,1)S(1)}, bf16[256,256]{1,0:T(8,128)(2,1)}, u32[]{:S(2)}) copy-start(bf16[256,256]{1,0:T(8,128)(2,1)} %constant.2.clone.pick) | copy-start | bytes 393220
  0.6 17.7 %copy-start = (bf16[2048,352]{0,1:T(8,128)(2,1)S(1)}, bf16[2048,352]{0,1:T(8,128)(2,1)}, u32[]{:S(2)}) copy-start(bf16[2048,352]{0,1:T(8,128)(2,1)} %param.10) | copy-start | bytes 4325380
  0.7 17.7 %copy-start.3 = (f32[2048]{0:T(1024)S(1)}, f32[2048]{0:T(1024)}, u32[]{:S(2)}) copy-start(f32[2048]{0:T(1024)} %param.9) | copy-start | bytes 24580
  14.6 3.8 %collective-permute-start = (bf16[64,4096]{1,0:T(8,128)(2,1)S(1)}, bf16[64,4096]{1,0:T(8,128)(2,1)S(1)}, u32[]{:S(2)}, u32[]{:S(2)}) collective-permute-start(bf16[64,4096]{1,0:T(8,128)(2,1)S(1)} %bitcast.6), channel_id=1, source_target_pairs={{0,1},{1,0},{2,3},{3,2},{4,5},{5,4},{6,7},{7,6},{8,9},{9,8},{10,11... | collective-permute-start | bytes 1572872 | tf_op jit(solution)/shard_map/ppermute | solution.py:208
  22.7 24.0 %all-to-all-start.1 = ((bf16[32,8,256]{2,1,0:T(8,128)(2,1)}), bf16[32,8,256]{2,1,0:T(8,128)(2,1)S(1)}, u32[]{:S(2)}, u32[]{:S(2)}) async-start(bf16[32,8,256]{2,1,0:T(8,128)(2,1)} %get-tuple-element.26), calls=%async_computation.1 | async-start | bytes 262144 | tf_op jit(solution)/shard_map/all_to_all | solution.py:255
  29.2 9.5 %collective-permute-start.5 = (bf16[128,896]{1,0:T(8,128)(2,1)S(1)}, bf16[128,896]{1,0:T(8,128)(2,1)S(1)}, u32[]{:S(2)}, u32[]{:S(2)}) collective-permute-start(bf16[128,896]{1,0:T(8,128)(2,1)S(1)} %get-tuple-element.23), channel_id=1, source_target_pairs={{0,8},{8,0},{16,24},{24,16},{32,40},{40,32},{48,56},{56,48},{64,72... | collective-permute-start | bytes 688136 | tf_op jit(solution)/shard_map/ppermute | solution.py:208
  32.6 14.2 %collective-permute-start.6 = (bf16[128,896]{1,0:T(8,128)(2,1)S(1)}, bf16[128,896]{1,0:T(8,128)(2,1)S(1)}, u32[]{:S(2)}, u32[]{:S(2)}) collective-permute-start(bf16[128,896]{1,0:T(8,128)(2,1)S(1)} %get-tuple-element.24), channel_id=1, source_target_pairs={{0,64},{8,72},{16,80},{24,88},{32,96},{40,104},{48,112},{56,120},{... | collective-permute-start | bytes 688136 | tf_op jit(solution)/shard_map/ppermute | solution.py:208
  36.1 10.7 %collective-permute-start.7 = (bf16[128,896]{1,0:T(8,128)(2,1)S(1)}, bf16[128,896]{1,0:T(8,128)(2,1)S(1)}, u32[]{:S(2)}, u32[]{:S(2)}) collective-permute-start(bf16[128,896]{1,0:T(8,128)(2,1)S(1)} %get-tuple-element.25), channel_id=1, source_target_pairs={{0,72},{8,64},{16,88},{24,80},{32,104},{40,96},{48,120},{56,112},{... | collective-permute-start | bytes 688136 | tf_op jit(solution)/shard_map/ppermute | solution.py:208
  46.8 33.0 %copy-start.1 = (bf16[16,2048]{1,0:T(8,128)(2,1)S(1)}, bf16[16,2048]{1,0:T(8,128)(2,1)}, u32[]{:S(2)}) copy-start(bf16[16,2048]{1,0:T(8,128)(2,1)} %inputs.1) | copy-start | bytes 196612
  48.2 32.4 %all-to-all-start.2 = ((bf16[16,104,128]{2,1,0:T(8,128)(2,1)}), bf16[16,104,128]{2,1,0:T(8,128)(2,1)S(1)}, u32[]{:S(2)}, u32[]{:S(2)}) async-start(bf16[16,104,128]{2,1,0:T(8,128)(2,1)} %shard_map.97), calls=%async_computation.2 | async-start | bytes 851968 | tf_op jit(solution)/shard_map/all_to_all | solution.py:270
  63.1 3.4 %collective-permute-start.1 = (bf16[64,2048]{1,0:T(8,128)(2,1)S(1)}, bf16[64,2048]{1,0:T(8,128)(2,1)S(1)}, u32[]{:S(2)}, u32[]{:S(2)}) collective-permute-start(bf16[64,2048]{1,0:T(8,128)(2,1)S(1)} %get-tuple-element.17), channel_id=1, source_target_pairs={{0,1},{1,0},{2,3},{3,2},{4,5},{5,4},{6,7},{7,6},{8,9},{9,8},{10,11... | collective-permute-start | bytes 786440 | tf_op jit(solution)/shard_map/ppermute | solution.py:208
  66.6 10.4 %collective-permute-start.2 = (bf16[16,2048]{1,0:T(8,128)(2,1)S(1)}, bf16[16,2048]{1,0:T(8,128)(2,1)S(1)}, u32[]{:S(2)}, u32[]{:S(2)}) collective-permute-start(bf16[16,2048]{1,0:T(8,128)(2,1)S(1)} %get-tuple-element.19), channel_id=1, source_target_pairs={{0,2},{2,0},{4,6},{6,4},{1,3},{3,1},{5,7},{7,5},{8,10},{10,8},{12,... | collective-permute-start | bytes 196616 | tf_op jit(solution)/shard_map/ppermute | solution.py:208
  68.5 8.5 %collective-permute-start.3 = (bf16[16,2048]{1,0:T(8,128)(2,1)S(1)}, bf16[16,2048]{1,0:T(8,128)(2,1)S(1)}, u32[]{:S(2)}, u32[]{:S(2)}) collective-permute-start(bf16[16,2048]{1,0:T(8,128)(2,1)S(1)} %get-tuple-element.20), channel_id=1, source_target_pairs={{0,4},{2,6},{4,0},{6,2},{1,5},{3,7},{5,1},{7,3},{8,12},{10,14},{12... | collective-permute-start | bytes 196616 | tf_op jit(solution)/shard_map/ppermute | solution.py:208
  72.4 7.4 %collective-permute-start.4 = (bf16[16,2048]{1,0:T(8,128)(2,1)S(1)}, bf16[16,2048]{1,0:T(8,128)(2,1)S(1)}, u32[]{:S(2)}, u32[]{:S(2)}) collective-permute-start(bf16[16,2048]{1,0:T(8,128)(2,1)S(1)} %get-tuple-element.21), channel_id=1, source_target_pairs={{0,6},{2,4},{4,2},{6,0},{1,7},{3,5},{5,3},{7,1},{8,14},{10,12},{12... | collective-permute-start | bytes 196616 | tf_op jit(solution)/shard_map/ppermute | solution.py:208
